TPU v7x, 768 devices: a whole 4x8x12 slice. The times are simulated.
768 devices in a mesh: sp: 12 (over z), tp: 8 (over y), dp: 8 (over x, core).
Axes of the slice: x: 4, y: 8, z: 12, core: 2. Of those that a mesh axis runs over, the one named last changes fastest.
Arguments:
- latent: bfloat16 [30720, 3072], P(('dp', 'sp', 'tp')), parts along dimension 0, may hold values from -6 to 6
- condition: float32 [24576], P('dp'), parts along dimension 0, may hold values from -8 to 8
- ctx_condition: float32 [3072], replicated, may hold values from -8 to 8
- context: bfloat16 [3072, 3072], P(('dp', 'sp')), parts along dimension 0, may hold values from -6 to 6
- mod_shift: bfloat16 [3072, 3072], P('sp', 'tp'), may hold values from -0.109375 to 0.109375
- mod_scale: bfloat16 [3072, 3072], P('sp', 'tp'), may hold values from -0.109375 to 0.109375
- mod_gate: bfloat16 [3072, 3072], P('sp', 'tp'), may hold values from -0.109375 to 0.109375
- norm_gain: float32 [3072], replicated, may hold values from 0.5 to 6
- w_query: bfloat16 [3072, 3072], P(None, 'tp'), may hold values from -0.109375 to 0.109375
- key_weight: bfloat16 [3072, 512], P(None, 'tp'), may hold values from -0.109375 to 0.109375
- value_weight: bfloat16 [3072, 512], P(None, 'tp'), may hold values from -0.109375 to 0.109375
- w_gate: bfloat16 [3072, 3072], P(None, 'tp'), may hold values from -0.109375 to 0.109375
- w_out: bfloat16 [3072, 3072], P('tp'), may hold values from -1.5 to 1.5
- sink_logit: float32 [48], P('tp'), may hold values from 4 to 7.5
Outputs:
- updated_latent: bfloat16 [30720, 3072], P(('dp', 'sp', 'tp')), parts along dimension 0
There are 8 independent parts, one for each index of `dp`. A program takes and returns all parts, laid end to end along the dimension named above; an argument that names none is the same for every part. Nothing has to cross between parts.
All inputs are finite; a program needn't handle non-finite values.
Results may differ from a plain program's by a relative error of at most 0.02.
The roundings to bfloat16 on the way count: a program that leaves them out, or rounds other values in their place, can miss the bound.
Values may be sent and summed in bfloat16 or wider, within the bound.
No kernel may reach another device: no remote copies, remote signals or barrier semaphores. Data moves between devices by JAX's collectives and lax.ppermute only.
A program may use at most 64 MiB of HBM per device.

v0:
```python
import functools
import math

import jax
import jax.numpy as jnp
from jax import lax
from jax.experimental import pallas as pl
from jax.experimental.pallas import tpu as pltpu
from jax.sharding import PartitionSpec as P

HEAD_SIZE = 64
WINDOW = 128
GRID_W = 64
LANES = 128
NORM_EPS = 1e-06
MASK_VALUE = -1e30
VMEM = pl.BlockSpec(memory_space=pltpu.VMEM)
HBM = pl.BlockSpec(memory_space=pltpu.HBM)
SMEM = pl.BlockSpec(memory_space=pltpu.SMEM)


def rounded(values):
    return values.astype(jnp.bfloat16)


def contract(left, right, right_dim=0):
    return lax.dot_general(
        left, right, (((1,), (right_dim,)), ((), ())), preferred_element_type=jnp.float32
    )


def call(kernel, out_shape, *operands, specs=None, scratch=(), flops=10**9, grant=30):
    return pl.pallas_call(
        kernel,
        out_shape=out_shape,
        in_specs=specs or [VMEM] * len(operands),
        out_specs=jax.tree.map(lambda _: VMEM, out_shape),
        scratch_shapes=scratch,
        compiler_params=pltpu.CompilerParams(vmem_limit_bytes=grant * 2**20),
        cost_estimate=pl.CostEstimate(flops=flops, bytes_accessed=10**6, transcendentals=0),
    )(*operands)


def row_offsets(own, count):
    direction = 1 - 2 * lax.rem(lax.axis_index("dp"), 2)
    rank = lax.axis_index("tp") + count
    behind = (count - 1) // 2
    return [
        lax.rem(rank + direction * distance, count) * own
        for distance in range(-behind, count - behind)
    ]


def partial_kernel(*refs, own):
    condition, ctx_condition, shift, scale, gate, out, cosine, sine = refs[:8]
    both, held, ready = refs[8:]
    fetches = [
        pltpu.make_async_copy(condition, both.at[0], ready.at[0]),
        pltpu.make_async_copy(ctx_condition, both.at[1], ready.at[1]),
    ]
    for index, weight in enumerate((shift, scale, gate)):
        fetches.append(pltpu.make_async_copy(weight, held.at[index], ready.at[2 + index]))
    for fetch in fetches:
        fetch.start()
    rows = cosine.shape[0]
    count = rows // own
    quarter = HEAD_SIZE // 4
    lane = lax.broadcasted_iota(jnp.int32, (own, LANES), 1)
    row = lax.broadcasted_iota(jnp.int32, (own, LANES), 0)
    entry = lane % (2 * quarter)
    inverse = jnp.exp(-math.log(10000.0) * (entry % quarter).astype(jnp.float32) / quarter)
    sign = jnp.where(lane % HEAD_SIZE < HEAD_SIZE // 2, -1.0, 1.0)
    begin = lax.axis_index("sp") * rows
    for index, offset in enumerate(row_offsets(own, count)):
        token = begin + offset + row
        angle = (
            jnp.where(entry < quarter, token // GRID_W, token % GRID_W).astype(jnp.float32)
            * inverse
        )
        cosine[index * own : (index + 1) * own, :] = jnp.cos(angle)
        sine[index * own : (index + 1) * own, :] = jnp.sin(angle) * sign
    for fetch in fetches[:2]:
        fetch.wait()
    size = held.shape[1]
    mine = pl.ds(pl.multiple_of(lax.axis_index("sp") * size, size), size)
    values = jnp.stack([both[0, mine], both[1, mine]])
    acts = rounded(values / (1.0 + jnp.exp(-values)))
    sums = []
    for index, fetch in enumerate(fetches[2:]):
        fetch.wait()
        sums.append(contract(acts, held[index]))
    sums = jnp.concatenate([sums[0], sums[1], sums[2][:1]], axis=0)
    for copy in range(out.shape[0]):
        out[copy] = sums


def total_kernel(parts, out):
    total = parts[0]
    for index in range(1, parts.shape[0]):
        total = total + parts[index]
    for copy in range(out.shape[0]):
        out[copy] = total


def modulated(pieces, vectors, gain, shift_row, scale_row, store):
    blocks, _, width = vectors.shape
    for read in pieces:
        square = None
        for block in range(blocks):
            values = read(block * width, width)
            part = sum(
                values[:, lane : lane + LANES] * values[:, lane : lane + LANES]
                for lane in range(0, width, LANES)
            )
            square = part if square is None else square + part
        mean = jnp.sum(square, axis=1, keepdims=True) / (blocks * width)
        inverse = lax.rsqrt(mean + NORM_EPS)
        for block in range(blocks):
            values = read(block * width, width)
            factor = gain[:, block * width : (block + 1) * width] * (
                1.0 + vectors[block, scale_row : scale_row + 1, :]
            )
            moved = values * inverse * factor + vectors[block, shift_row : shift_row + 1, :]
            store(read, block * width, rounded(moved))


def context_kernel(context, vectors, gain, key_weight, value_weight, out, hidden):
    def store(_, column, rows):
        hidden[:, column : column + rows.shape[1]] = rows

    modulated([lambda c, n: context[:, c : c + n].astype(jnp.float32)], vectors, gain, 1, 3, store)
    weight = jnp.concatenate([key_weight[...], value_weight[...]], axis=0)
    pair = rounded(contract(hidden[...], weight, 1))
    for copy in range(out.shape[0]):
        out[copy] = pair


def turned(values, cosine, sine):
    lane = lax.broadcasted_iota(jnp.int32, values.shape, 1)
    half = HEAD_SIZE // 2
    other = jnp.where(
        lane % HEAD_SIZE < half, pltpu.roll(values, LANES - half, 1), pltpu.roll(values, half, 1)
    )
    return values * cosine + other * sine


def key_kernel(*refs, pieces, per_group):
    count = sum(len(piece) for piece in pieces)
    blocks = list(refs[:count])
    vectors, gain, key_weight, value_weight, cosine, sine = refs[count : 6 + count]
    hidden, key_value, first, last, ordered = refs[6 + count :]
    own = hidden.shape[0] // len(pieces)
    members = [[blocks.pop(0) for _ in piece] for piece in pieces]
    reads, places = [], {}
    for group in range(0, len(members), per_group):

        def read(column, columns, parts=members[group : group + per_group]):
            rows = []
            for part in parts:
                held = part[0].shape[1]
                ref, at = part[column // held], column % held
                rows.append(ref[:, at : at + columns].astype(jnp.float32))
            return jnp.concatenate(rows, axis=0) if len(rows) > 1 else rows[0]

        reads.append(read)
        places[read] = group * own

    def store(read, column, rows):
        begin = places[read]
        hidden[begin : begin + rows.shape[0], column : column + rows.shape[1]] = rows

    modulated(reads, vectors, gain, 0, 2, store)
    weight = jnp.concatenate([key_weight[...], value_weight[...]], axis=0)
    both = contract(hidden[...], weight, 1)
    lane = lax.broadcasted_iota(jnp.int32, both.shape, 1)
    both = jnp.where(lane < HEAD_SIZE, turned(both, cosine[...], sine[...]), both)
    for index, offset in enumerate(row_offsets(own, len(pieces))):
        begin = pl.multiple_of(offset, 8)
        ordered[pl.ds(begin, own), :] = both[index * own : (index + 1) * own, :]
    key_value[...] = rounded(ordered[...])
    first[...] = rounded(ordered[:WINDOW, :])
    last[...] = rounded(ordered[ordered.shape[0] - WINDOW :, :])


def query_kernel(hidden, w_query, w_gate, cosine, sine, queries, gate, held, ready, *, own):
    fetch = pltpu.make_async_copy(w_gate, held, ready)
    fetch.start()
    rows, width = hidden.shape[0], w_query.shape[1]
    projected = contract(hidden[...], w_query[...])
    heads = width // HEAD_SIZE
    lane = lax.broadcasted_iota(jnp.int32, (rows, LANES), 1)
    for pair in range(width // LANES):
        tile = turned(projected[:, pair * LANES : (pair + 1) * LANES], cosine[...], sine[...])
        tile = tile * (1.0 / math.sqrt(HEAD_SIZE))
        for odd in range(2):
            head = 2 * pair + odd
            aligned = pltpu.roll(tile, HEAD_SIZE, 1) if odd else tile
            aligned = jnp.where(lane < HEAD_SIZE, aligned, 0.0)
            for block in range(rows // own):
                begin = (block * heads + head) * own
                queries[begin : begin + own, :] = aligned[block * own : (block + 1) * own, :]
    fetch.wait()
    gate[...] = rounded(contract(hidden[...], held[...])).astype(jnp.float32)


def attend_kernel(
    sink,
    queries,
    gate,
    low,
    middle,
    high,
    ctx,
    w_out,
    out,
    padded,
    mixed,
    held,
    ready,
    *,
    own,
    span,
):
    fetch = pltpu.make_async_copy(w_out, held, ready)
    fetch.start()
    rows = middle.shape[0]
    width = w_out.shape[0]
    heads = width // HEAD_SIZE
    padded[:WINDOW, :] = low[...].astype(jnp.float32)
    padded[WINDOW : WINDOW + rows, :] = middle[...].astype(jnp.float32)
    padded[WINDOW + rows : 2 * WINDOW + rows, :] = high[...].astype(jnp.float32)
    padded[2 * WINDOW + rows :, :] = jnp.zeros_like(padded[2 * WINDOW + rows :, :])
    row = lax.broadcasted_iota(jnp.int32, (own, span), 0)
    column = lax.broadcasted_iota(jnp.int32, (own, span), 1)
    in_reach = (column >= row) & (column <= row + 2 * WINDOW)
    lane = lax.broadcasted_iota(jnp.int32, (own, LANES), 1)
    sinks = jnp.concatenate([jnp.full((own, 1), sink[h], jnp.float32) for h in range(heads)], axis=0)
    begin = lax.axis_index("sp") * rows
    total = lax.axis_size("sp") * rows
    for block, offset in enumerate(row_offsets(own, rows // own)):
        offset = pl.multiple_of(offset, 8)
        near = rounded(padded[pl.ds(offset, span), :])
        query = rounded(queries[block * heads * own : (block + 1) * heads * own, :])
        near_scores = contract(query, near, 1)
        ctx_scores = contract(query, ctx[...], 1)
        token = begin - WINDOW + offset + column
        seen = in_reach & (token >= 0) & (token < total)
        near_scores = jnp.where(
            seen[None], near_scores.reshape(heads, own, span), MASK_VALUE
        ).reshape(heads * own, span)
        peak = jnp.maximum(
            jnp.maximum(
                jnp.max(near_scores, axis=1, keepdims=True),
                jnp.max(ctx_scores, axis=1, keepdims=True),
            ),
            sinks,
        )
        near_exp = jnp.exp(near_scores - peak)
        ctx_exp = jnp.exp(ctx_scores - peak)
        denominator = (
            jnp.sum(near_exp, axis=1, keepdims=True)
            + jnp.sum(ctx_exp, axis=1, keepdims=True)
            + jnp.exp(sinks - peak)
        )
        inverse = 1.0 / denominator
        result = contract(rounded(near_exp * inverse), near) + contract(
            rounded(ctx_exp * inverse), ctx[...]
        )
        here = slice(block * own, (block + 1) * own)
        for pair in range(heads // 2):
            even = result[2 * pair * own : (2 * pair + 1) * own, :]
            odd = result[(2 * pair + 1) * own : (2 * pair + 2) * own, :]
            attended = jnp.where(lane < HEAD_SIZE, pltpu.roll(even, HEAD_SIZE, 1), odd)
            tile = gate[here, pair * LANES : (pair + 1) * LANES]
            mixed[here, pair * LANES : (pair + 1) * LANES] = attended * (
                tile / (1.0 + jnp.exp(-tile))
            )
    fetch.wait()
    final = rounded(mixed[...])
    step = 512
    for begin in range(0, w_out.shape[1], step):
        out[:, begin : begin + step] = rounded(contract(final, held[:, begin : begin + step]))


def copy_for_each(copies, axis):
    return lax.all_to_all(copies, axis, split_axis=0, concat_axis=0, tiled=True)


def shift(block, axis, steps, wrap=True):
    count = lax.axis_size(axis)
    pairs = [(i, (i + steps) % count) for i in range(count) if wrap or 0 <= i + steps < count]
    return lax.ppermute(block, axis, pairs)


def added(first, *others):
    total = first.astype(jnp.float32)
    for other in others:
        total = total + other.astype(jnp.float32)
    return rounded(total)


def toward(block, steps):
    tp_count, dp_count = lax.axis_size("tp"), lax.axis_size("dp")
    pairs = []
    for i in range(tp_count):
        for j in range(dp_count):
            target = (i + (steps if j % 2 == 0 else -steps)) % tp_count
            pairs.append((i * dp_count + j, target * dp_count + j))
    return lax.ppermute(block, ("tp", "dp"), pairs)


def gather_rows(latent):
    back2 = toward(latent, 2)
    ahead2 = toward(latent, -2)
    back1 = toward(latent, 1)
    ahead1 = toward(latent, -1)
    far = toward(back2, 2)
    back3, ahead3 = toward(back2, 1), toward(ahead2, -1)
    return [(back3,), (back2,), (back1,), (latent,), (ahead1,), (ahead2,), (ahead3,), (far,)]


def reduce_rows(block):
    far = toward(block(4), 2)
    down3 = toward(block(-3), -1)
    up3 = toward(block(3), 1)
    minus_two = added(block(-2), down3)
    down2 = toward(minus_two, -2)
    ahead, _ = lax.optimization_barrier((block(2), minus_two))
    up2 = toward(added(ahead, up3, far), 2)
    up1 = toward(block(1), 1)
    down1 = toward(block(-1), -1)
    total = block(0).astype(jnp.float32)
    for part in (up1, down1, up2, down2):
        total = total + part.astype(jnp.float32)
    return total


def body(
    latent,
    condition,
    ctx_condition,
    context,
    mod_shift,
    mod_scale,
    mod_gate,
    norm_gain,
    w_query,
    key_weight,
    value_weight,
    w_gate,
    w_out,
    sink_logit,
):
    f32, bf16 = jnp.float32, jnp.bfloat16
    shape = jax.ShapeDtypeStruct
    sp_count, tp_count = lax.axis_size("sp"), lax.axis_size("tp")
    own, width = latent.shape
    rows = own * tp_count
    mod_rows, columns = mod_shift.shape
    behind = (tp_count - 1) // 2

    parts, cosine, sine = call(
        functools.partial(partial_kernel, own=own),
        [
            shape((sp_count, 5, columns), f32),
            shape((rows, LANES), f32),
            shape((rows, LANES), f32),
        ],
        condition,
        ctx_condition,
        mod_shift,
        mod_scale,
        mod_gate,
        specs=[HBM] * 5,
        scratch=[
            pltpu.VMEM((2, *condition.shape), f32),
            pltpu.VMEM((3, mod_rows, columns), bf16),
            pltpu.SemaphoreType.DMA((5,)),
        ],
        grant=62,
    )
    pieces = gather_rows(latent)
    parts = copy_for_each(parts, "sp")
    totals = call(total_kernel, shape((tp_count, 5, columns), f32), parts, grant=30)
    vectors = copy_for_each(totals, "tp")

    gain = norm_gain[None, :]
    kv_weights = (key_weight.T, value_weight.T)
    ctx_rows = context.shape[0]
    ctx_pair = call(
        context_kernel,
        shape((sp_count, ctx_rows, LANES), bf16),
        context,
        vectors,
        gain,
        *kv_weights,
        scratch=[pltpu.VMEM((ctx_rows, width), bf16)],
        grant=30,
    )
    ctx_all = copy_for_each(ctx_pair, "sp").reshape(sp_count * ctx_rows, LANES)

    blocks = [block for piece in pieces for block in piece]
    hidden, key_value, first, last = call(
        functools.partial(key_kernel, pieces=[[0] * len(p) for p in pieces], per_group=2),
        [
            shape((rows, width), bf16),
            shape((rows, LANES), bf16),
            shape((WINDOW, LANES), bf16),
            shape((WINDOW, LANES), bf16),
        ],
        *blocks,
        vectors,
        gain,
        *kv_weights,
        cosine,
        sine,
        scratch=[pltpu.VMEM((rows, LANES), f32)],
        grant=30,
    )
    low = shift(last, "sp", 1, wrap=False)
    high = shift(first, "sp", -1, wrap=False)
    heads = w_query.shape[1] // HEAD_SIZE
    queries, gate = call(
        functools.partial(query_kernel, own=own),
        [shape((rows * heads, LANES), f32), shape((rows, w_gate.shape[1]), f32)],
        hidden,
        w_query,
        w_gate,
        cosine,
        sine,
        specs=[VMEM, VMEM, HBM, VMEM, VMEM],
        scratch=[pltpu.VMEM(w_gate.shape, bf16), pltpu.SemaphoreType.DMA],
        flops=2 * 10**9,
        grant=46,
    )
    span = 3 * LANES
    product = call(
        functools.partial(attend_kernel, own=own, span=span),
        shape((rows, width), bf16),
        sink_logit,
        queries,
        gate,
        low,
        key_value,
        high,
        ctx_all,
        w_out,
        specs=[SMEM] + [VMEM] * 6 + [HBM],
        scratch=[
            pltpu.VMEM((rows - own + span, LANES), f32),
            pltpu.VMEM((rows, w_out.shape[0]), f32),
            pltpu.VMEM(w_out.shape, bf16),
            pltpu.SemaphoreType.DMA,
        ],
        flops=3 * 10**9,
        grant=50,
    )
    branch = reduce_rows(lambda d: product[(d + behind) * own : (d + behind + 1) * own])
    lat_gate = vectors[:, 4, :].reshape(width)
    return rounded(latent.astype(f32) + lat_gate * branch)


def solution(mesh):
    return jax.shard_map(
        body,
        mesh=mesh,
        in_specs=(
            P(("dp", "sp", "tp"), None),
            P("dp"),
            P(),
            P(("dp", "sp"), None),
            P("sp", "tp"),
            P("sp", "tp"),
            P("sp", "tp"),
            P(),
            P(None, "tp"),
            P(None, "tp"),
            P(None, "tp"),
            P(None, "tp"),
            P("tp", None),
            P("tp"),
        ),
        out_specs=P(("dp", "sp", "tp"), None),
        check_vma=False,
    )
```

profile of v0, /device:TPU:52, one launch (start us, length us, event | category | flops | bytes accessed | tf_op | source)
XLA Modules:
  0.0 124.7 jit_solution(18008300812767591474)
XLA Ops:
  0.0 2.2 %shard_map.136 = (f32[12,5,384]{2,1,0:T(8,128)}, f32[320,128]{1,0:T(8,128)}, f32[320,128]{1,0:T(8,128)}) custom-call(f32[3072]{0:T(1024)} %refs_0_.1, f32[3072]{0:T(1024)} %refs_1_.1, bf16[256,384]{1,0:T(8,128)(2,1)} %refs_2_.1, bf16[256,384]{1,0:T(8,128)(2,1)} %refs_3_.2, bf16[256,384]{1,0:T(8,128)(2,1)} %refs_4_.1), custom_call_target="tpu_custom_call" | custom-call | flops 1000000000 | bytes 1000000 | tf_op jit(solution)/shard_map/pallas_call | solution.py:33
  2.2 15.2 %all-to-all-start = ((f32[12,5,384]{2,1,0:T(8,128)}), f32[12,5,384]{2,1,0:T(8,128)S(1)}, u32[]{:S(2)}, u32[]{:S(2)}) async-start(f32[12,5,384]{2,1,0:T(8,128)} %get-tuple-element.15), calls=%async_computation | async-start | bytes 294912 | tf_op jit(solution)/shard_map/all_to_all | solution.py:286
  17.4 2.1 %collective-permute-start = (bf16[40,3072]{1,0:T(8,128)(2,1)S(1)}, bf16[40,3072]{1,0:T(8,128)(2,1)S(1)}, u32[]{:S(2)}, u32[]{:S(2)}) collective-permute-start(bf16[40,3072]{1,0:T(8,128)(2,1)S(1)} %copy-done), channel_id=1, source_target_pairs={{0,16},{1,49},{2,18},{3,51},{4,20},{5,53},{6,22},{7,55},{8,24},{9,... | collective-permute-start | bytes 737288 | tf_op jit(solution)/shard_map/ppermute | solution.py:309
  19.5 4.8 %collective-permute-start.4 = (bf16[40,3072]{1,0:T(8,128)(2,1)S(1)}, bf16[40,3072]{1,0:T(8,128)(2,1)S(1)}, u32[]{:S(2)}, u32[]{:S(2)}) collective-permute-start(bf16[40,3072]{1,0:T(8,128)(2,1)S(1)} %copy-done), channel_id=1, source_target_pairs={{0,48},{1,17},{2,50},{3,19},{4,52},{5,21},{6,54},{7,23},{8,56},{9,... | collective-permute-start | bytes 737288 | tf_op jit(solution)/shard_map/ppermute | solution.py:309
  24.3 2.6 %collective-permute-start.2 = (bf16[40,3072]{1,0:T(8,128)(2,1)S(1)}, bf16[40,3072]{1,0:T(8,128)(2,1)S(1)}, u32[]{:S(2)}, u32[]{:S(2)}) collective-permute-start(bf16[40,3072]{1,0:T(8,128)(2,1)S(1)} %copy-done), channel_id=1, source_target_pairs={{0,8},{1,57},{2,10},{3,59},{4,12},{5,61},{6,14},{7,63},{8,16},{9,1... | collective-permute-start | bytes 737288 | tf_op jit(solution)/shard_map/ppermute | solution.py:309
  26.9 3.8 %collective-permute-start.3 = (bf16[40,3072]{1,0:T(8,128)(2,1)S(1)}, bf16[40,3072]{1,0:T(8,128)(2,1)S(1)}, u32[]{:S(2)}, u32[]{:S(2)}) collective-permute-start(bf16[40,3072]{1,0:T(8,128)(2,1)S(1)} %copy-done), channel_id=1, source_target_pairs={{0,56},{1,9},{2,58},{3,11},{4,60},{5,13},{6,62},{7,15},{8,0},{9,17... | collective-permute-start | bytes 737288 | tf_op jit(solution)/shard_map/ppermute | solution.py:309
  30.7 4.7 %collective-permute-start.1 = (bf16[40,3072]{1,0:T(8,128)(2,1)S(1)}, bf16[40,3072]{1,0:T(8,128)(2,1)S(1)}, u32[]{:S(2)}, u32[]{:S(2)}) collective-permute-start(bf16[40,3072]{1,0:T(8,128)(2,1)S(1)} %collective-permute-done.refs_1_), channel_id=1, source_target_pairs={{0,8},{1,57},{2,10},{3,59},{4,12},{5,61},{6,14},{7,63},{8,16},{9,1... | collective-permute-start | bytes 737288 | tf_op jit(solution)/shard_map/ppermute | solution.py:309
  35.4 4.1 %collective-permute-start.6 = (bf16[40,3072]{1,0:T(8,128)(2,1)S(1)}, bf16[40,3072]{1,0:T(8,128)(2,1)S(1)}, u32[]{:S(2)}, u32[]{:S(2)}) collective-permute-start(bf16[40,3072]{1,0:T(8,128)(2,1)S(1)} %collective-permute-done.refs_1_), channel_id=1, source_target_pairs={{0,16},{1,49},{2,18},{3,51},{4,20},{5,53},{6,22},{7,55},{8,24},{9,... | collective-permute-start | bytes 737288 | tf_op jit(solution)/shard_map/ppermute | solution.py:309
  39.5 1.9 %collective-permute-start.5 = (bf16[40,3072]{1,0:T(8,128)(2,1)S(1)}, bf16[40,3072]{1,0:T(8,128)(2,1)S(1)}, u32[]{:S(2)}, u32[]{:S(2)}) collective-permute-start(bf16[40,3072]{1,0:T(8,128)(2,1)S(1)} %collective-permute-done.4.refs_5_), channel_id=1, source_target_pairs={{0,56},{1,9},{2,58},{3,11},{4,60},{5,13},{6,62},{7,15},{8,0},{9,17... | collective-permute-start | bytes 737288 | tf_op jit(solution)/shard_map/ppermute | solution.py:309
  41.5 14.4 %all_to_all.15.refs_8_.vectors = f32[8,5,384]{2,1,0:T(8,128)S(1)} all-to-all(f32[8,5,384]{2,1,0:T(8,128)S(1)} %shard_map.137), channel_id=1, replica_groups=mesh['sp'=12,'tp'=8,'dp'=8] {'tp'}, dimensions={0} | all-to-all | bytes 122880 | tf_op jit(solution)/shard_map/all_to_all | solution.py:286
  57.0 9.7 %all-to-all-start.2 = ((bf16[12,32,128]{2,1,0:T(8,128)(2,1)}), bf16[12,32,128]{2,1,0:T(8,128)(2,1)S(1)}, u32[]{:S(2)}, u32[]{:S(2)}) async-start(bf16[12,32,128]{2,1,0:T(8,128)(2,1)} %shard_map.140), calls=%async_computation.2 | async-start | bytes 196608 | tf_op jit(solution)/shard_map/all_to_all | solution.py:286
  68.3 3.9 %collective-permute-start.7 = (bf16[128,128]{1,0:T(8,128)(2,1)S(1)}, bf16[128,128]{1,0:T(8,128)(2,1)S(1)}, u32[]{:S(2)}, u32[]{:S(2)}) collective-permute-start(bf16[128,128]{1,0:T(8,128)(2,1)S(1)} %get-tuple-element.21), channel_id=1, source_target_pairs={{0,64},{64,128},{128,192},{192,256},{256,320},{320,384},{384,448},... | collective-permute-start | bytes 98312 | tf_op jit(solution)/shard_map/ppermute | solution.py:292
  73.5 2.9 %shard_map.139 = (f32[1920,128]{1,0:T(8,128)S(1)}, f32[320,384]{1,0:T(8,128)S(1)}) custom-call(bf16[320,3072]{1,0:T(8,128)(2,1)S(1)} %get-tuple-element.18.hidden, bf16[3072,384]{1,0:T(8,128)(2,1)S(1)} %copy-done.1, bf16[3072,384]{1,0:T(8,128)(2,1)} %w_gate.1, f32[320,128]{1,0:T(8,128)S(1)} %copy-done.7, f32[320,128]{1,0:T(8,128)S(1)} %copy-done.8), custom_call_target="tpu_custom_call" | custom-call | flops 2000000000 | bytes 1000000 | tf_op jit(solution)/shard_map/pallas_call | solution.py:33
  76.4 1.6 %collective-permute-done.8.high = bf16[128,128]{1,0:T(8,128)(2,1)S(1)} collective-permute-done((bf16[128,128]{1,0:T(8,128)(2,1)S(1)}, bf16[128,128]{1,0:T(8,128)(2,1)S(1)}, u32[]{:S(2)}, u32[]{:S(2)}) %collective-permute-start.8) | collective-permute-done | bytes 32800 | tf_op jit(solution)/shard_map/ppermute | solution.py:292
  78.4 7.9 %shard_map.141 = bf16[320,3072]{1,0:T(8,128)(2,1)S(1)} custom-call(f32[6]{0:T(128)S(1)} %copy-done.6, f32[1920,128]{1,0:T(8,128)S(1)} %get-tuple-element.19.queries, f32[320,384]{1,0:T(8,128)S(1)} %get-tuple-element.20.gate, bf16[128,128]{1,0:T(8,128)(2,1)S(1)} %collective-permute-done.7.low, bf16[320,128]{1,0:T(8,128)(2,1)S(1)} %get-tuple-element.22.middle, ...), custom_call_target="tpu_custom_call" | custom-call | flops 3000000000 | bytes 1000000 | tf_op jit(solution)/shard_map/pallas_call | solution.py:33
  86.4 2.6 %collective-permute-start.11 = (bf16[40,3072]{1,0:T(8,128)(2,1)S(1)}, bf16[40,3072]{1,0:T(8,128)(2,1)S(1)}, u32[]{:S(2)}, u32[]{:S(2)}) collective-permute-start(bf16[40,3072]{1,0:T(8,128)(2,1)S(1)} %get-tuple-element.28), channel_id=1, source_target_pairs={{0,56},{1,9},{2,58},{3,11},{4,60},{5,13},{6,62},{7,15},{8,0},{9,17... | collective-permute-start | bytes 737288 | tf_op jit(solution)/shard_map/ppermute | solution.py:309
  89.0 3.2 %collective-permute-start.12 = (bf16[40,3072]{1,0:T(8,128)(2,1)S(1)}, bf16[40,3072]{1,0:T(8,128)(2,1)S(1)}, u32[]{:S(2)}, u32[]{:S(2)}) collective-permute-start(bf16[40,3072]{1,0:T(8,128)(2,1)S(1)} %get-tuple-element.27), channel_id=1, source_target_pairs={{0,8},{1,57},{2,10},{3,59},{4,12},{5,61},{6,14},{7,63},{8,16},{9,1... | collective-permute-start | bytes 737288 | tf_op jit(solution)/shard_map/ppermute | solution.py:309
  92.2 5.7 %collective-permute-start.13 = (bf16[40,3072]{1,0:T(8,128)(2,1)S(1)}, bf16[40,3072]{1,0:T(8,128)(2,1)S(1)}, u32[]{:S(2)}, u32[]{:S(2)}) collective-permute-start(bf16[40,3072]{1,0:T(8,128)(2,1)S(1)} %get-tuple-element.26), channel_id=1, source_target_pairs={{0,16},{1,49},{2,18},{3,51},{4,20},{5,53},{6,22},{7,55},{8,24},{9,... | collective-permute-start | bytes 737288 | tf_op jit(solution)/shard_map/ppermute | solution.py:309
  98.0 2.0 %collective-permute-start.10 = (bf16[40,3072]{1,0:T(8,128)(2,1)S(1)}, bf16[40,3072]{1,0:T(8,128)(2,1)S(1)}, u32[]{:S(2)}, u32[]{:S(2)}) collective-permute-start(bf16[40,3072]{1,0:T(8,128)(2,1)S(1)} %get-tuple-element.30), channel_id=1, source_target_pairs={{0,56},{1,9},{2,58},{3,11},{4,60},{5,13},{6,62},{7,15},{8,0},{9,17... | collective-permute-start | bytes 737288 | tf_op jit(solution)/shard_map/ppermute | solution.py:309
  99.9 3.9 %collective-permute-start.9 = (bf16[40,3072]{1,0:T(8,128)(2,1)S(1)}, bf16[40,3072]{1,0:T(8,128)(2,1)S(1)}, u32[]{:S(2)}, u32[]{:S(2)}) collective-permute-start(bf16[40,3072]{1,0:T(8,128)(2,1)S(1)} %get-tuple-element.25), channel_id=1, source_target_pairs={{0,8},{1,57},{2,10},{3,59},{4,12},{5,61},{6,14},{7,63},{8,16},{9,1... | collective-permute-start | bytes 737288 | tf_op jit(solution)/shard_map/ppermute | solution.py:309
  104.4 6.6 %collective-permute-start.14 = (bf16[40,3072]{1,0:T(8,128)(2,1)S(1)}, bf16[40,3072]{1,0:T(8,128)(2,1)S(1)}, u32[]{:S(2)}, u32[]{:S(2)}) collective-permute-start(bf16[40,3072]{1,0:T(8,128)(2,1)S(1)} %add_convert_fusion.1), channel_id=1, source_target_pairs={{0,16},{1,49},{2,18},{3,51},{4,20},{5,53},{6,22},{7,55},{8,24},{9,... | collective-permute-start | bytes 737288 | tf_op jit(solution)/shard_map/ppermute | solution.py:309
  111.0 1.9 %collective-permute-start.15 = (bf16[40,3072]{1,0:T(8,128)(2,1)S(1)}, bf16[40,3072]{1,0:T(8,128)(2,1)S(1)}, u32[]{:S(2)}, u32[]{:S(2)}) collective-permute-start(bf16[40,3072]{1,0:T(8,128)(2,1)S(1)} %add_convert_fusion.2), channel_id=1, source_target_pairs={{0,48},{1,17},{2,50},{3,19},{4,52},{5,21},{6,54},{7,23},{8,56},{9,... | collective-permute-start | bytes 737288 | tf_op jit(solution)/shard_map/ppermute | solution.py:309
  113.0 5.4 %collective-permute-done.14 = bf16[40,3072]{1,0:T(8,128)(2,1)S(1)} collective-permute-done((bf16[40,3072]{1,0:T(8,128)(2,1)S(1)}, bf16[40,3072]{1,0:T(8,128)(2,1)S(1)}, u32[]{:S(2)}, u32[]{:S(2)}) %collective-permute-start.14) | collective-permute-done | bytes 245792 | tf_op jit(solution)/shard_map/ppermute | solution.py:309
  118.4 5.4 %collective-permute-done.15 = bf16[40,3072]{1,0:T(8,128)(2,1)S(1)} collective-permute-done((bf16[40,3072]{1,0:T(8,128)(2,1)S(1)}, bf16[40,3072]{1,0:T(8,128)(2,1)S(1)}, u32[]{:S(2)}, u32[]{:S(2)}) %collective-permute-start.15) | collective-permute-done | bytes 245792 | tf_op jit(solution)/shard_map/ppermute | solution.py:309
  (42 shorter events, 5.9 us)
Async XLA Ops:
  0.0 17.3 %copy-start = (bf16[40,3072]{1,0:T(8,128)(2,1)S(1)}, bf16[40,3072]{1,0:T(8,128)(2,1)}, u32[]{:S(2)}) copy-start(bf16[40,3072]{1,0:T(8,128)(2,1)} %refs_3_.3) | copy-start | bytes 737284
  2.2 39.3 %all-to-all-start = ((f32[12,5,384]{2,1,0:T(8,128)}), f32[12,5,384]{2,1,0:T(8,128)S(1)}, u32[]{:S(2)}, u32[]{:S(2)}) async-start(f32[12,5,384]{2,1,0:T(8,128)} %get-tuple-element.15), calls=%async_computation | async-start | bytes 294912 | tf_op jit(solution)/shard_map/all_to_all | solution.py:286
  17.3 38.5 %copy-start.2 = (bf16[3072,64]{0,1:T(8,128)(2,1)S(1)}, bf16[3072,64]{0,1:T(8,128)(2,1)}, u32[]{:S(2)}) copy-start(bf16[3072,64]{0,1:T(8,128)(2,1)} %param.23) | copy-start | bytes 1179652
  17.4 38.5 %copy-start.3 = (bf16[3072,64]{0,1:T(8,128)(2,1)S(1)}, bf16[3072,64]{0,1:T(8,128)(2,1)}, u32[]{:S(2)}) copy-start(bf16[3072,64]{0,1:T(8,128)(2,1)} %param.24) | copy-start | bytes 1179652
  17.4 38.5 %copy-start.4 = (bf16[32,3072]{1,0:T(8,128)(2,1)S(1)}, bf16[32,3072]{1,0:T(8,128)(2,1)}, u32[]{:S(2)}) copy-start(bf16[32,3072]{1,0:T(8,128)(2,1)} %context.1) | copy-start | bytes 589828
  17.4 38.5 %copy-start.5 = (f32[3072]{0:T(1024)S(1)}, f32[3072]{0:T(1024)}, u32[]{:S(2)}) copy-start(f32[3072]{0:T(1024)} %param.21) | copy-start | bytes 36868
  17.4 13.3 %collective-permute-start = (bf16[40,3072]{1,0:T(8,128)(2,1)S(1)}, bf16[40,3072]{1,0:T(8,128)(2,1)S(1)}, u32[]{:S(2)}, u32[]{:S(2)}) collective-permute-start(bf16[40,3072]{1,0:T(8,128)(2,1)S(1)} %copy-done), channel_id=1, source_target_pairs={{0,16},{1,49},{2,18},{3,51},{4,20},{5,53},{6,22},{7,55},{8,24},{9,... | collective-permute-start | bytes 737288 | tf_op jit(solution)/shard_map/ppermute | solution.py:309
  19.5 20.0 %collective-permute-start.4 = (bf16[40,3072]{1,0:T(8,128)(2,1)S(1)}, bf16[40,3072]{1,0:T(8,128)(2,1)S(1)}, u32[]{:S(2)}, u32[]{:S(2)}) collective-permute-start(bf16[40,3072]{1,0:T(8,128)(2,1)S(1)} %copy-done), channel_id=1, source_target_pairs={{0,48},{1,17},{2,50},{3,19},{4,52},{5,21},{6,54},{7,23},{8,56},{9,... | collective-permute-start | bytes 737288 | tf_op jit(solution)/shard_map/ppermute | solution.py:309
  24.3 42.4 %collective-permute-start.2 = (bf16[40,3072]{1,0:T(8,128)(2,1)S(1)}, bf16[40,3072]{1,0:T(8,128)(2,1)S(1)}, u32[]{:S(2)}, u32[]{:S(2)}) collective-permute-start(bf16[40,3072]{1,0:T(8,128)(2,1)S(1)} %copy-done), channel_id=1, source_target_pairs={{0,8},{1,57},{2,10},{3,59},{4,12},{5,61},{6,14},{7,63},{8,16},{9,1... | collective-permute-start | bytes 737288 | tf_op jit(solution)/shard_map/ppermute | solution.py:309
  26.9 39.9 %collective-permute-start.3 = (bf16[40,3072]{1,0:T(8,128)(2,1)S(1)}, bf16[40,3072]{1,0:T(8,128)(2,1)S(1)}, u32[]{:S(2)}, u32[]{:S(2)}) collective-permute-start(bf16[40,3072]{1,0:T(8,128)(2,1)S(1)} %copy-done), channel_id=1, source_target_pairs={{0,56},{1,9},{2,58},{3,11},{4,60},{5,13},{6,62},{7,15},{8,0},{9,17... | collective-permute-start | bytes 737288 | tf_op jit(solution)/shard_map/ppermute | solution.py:309
  30.7 36.0 %collective-permute-start.1 = (bf16[40,3072]{1,0:T(8,128)(2,1)S(1)}, bf16[40,3072]{1,0:T(8,128)(2,1)S(1)}, u32[]{:S(2)}, u32[]{:S(2)}) collective-permute-start(bf16[40,3072]{1,0:T(8,128)(2,1)S(1)} %collective-permute-done.refs_1_), channel_id=1, source_target_pairs={{0,8},{1,57},{2,10},{3,59},{4,12},{5,61},{6,14},{7,63},{8,16},{9,1... | collective-permute-start | bytes 737288 | tf_op jit(solution)/shard_map/ppermute | solution.py:309
  35.4 31.3 %collective-permute-start.6 = (bf16[40,3072]{1,0:T(8,128)(2,1)S(1)}, bf16[40,3072]{1,0:T(8,128)(2,1)S(1)}, u32[]{:S(2)}, u32[]{:S(2)}) collective-permute-start(bf16[40,3072]{1,0:T(8,128)(2,1)S(1)} %collective-permute-done.refs_1_), channel_id=1, source_target_pairs={{0,16},{1,49},{2,18},{3,51},{4,20},{5,53},{6,22},{7,55},{8,24},{9,... | collective-permute-start | bytes 737288 | tf_op jit(solution)/shard_map/ppermute | solution.py:309
  39.5 27.3 %collective-permute-start.5 = (bf16[40,3072]{1,0:T(8,128)(2,1)S(1)}, bf16[40,3072]{1,0:T(8,128)(2,1)S(1)}, u32[]{:S(2)}, u32[]{:S(2)}) collective-permute-start(bf16[40,3072]{1,0:T(8,128)(2,1)S(1)} %collective-permute-done.4.refs_5_), channel_id=1, source_target_pairs={{0,56},{1,9},{2,58},{3,11},{4,60},{5,13},{6,62},{7,15},{8,0},{9,17... | collective-permute-start | bytes 737288 | tf_op jit(solution)/shard_map/ppermute | solution.py:309
  55.8 10.9 %copy-start.8 = (f32[320,128]{1,0:T(8,128)S(1)}, f32[320,128]{1,0:T(8,128)}, u32[]{:S(2)}) copy-start(f32[320,128]{1,0:T(8,128)} %get-tuple-element.17.refs_13_.sine) | copy-start | bytes 491524
  57.0 21.4 %all-to-all-start.2 = ((bf16[12,32,128]{2,1,0:T(8,128)(2,1)}), bf16[12,32,128]{2,1,0:T(8,128)(2,1)S(1)}, u32[]{:S(2)}, u32[]{:S(2)}) async-start(bf16[12,32,128]{2,1,0:T(8,128)(2,1)} %shard_map.140), calls=%async_computation.2 | async-start | bytes 196608 | tf_op jit(solution)/shard_map/all_to_all | solution.py:286
  68.3 8.1 %collective-permute-start.7 = (bf16[128,128]{1,0:T(8,128)(2,1)S(1)}, bf16[128,128]{1,0:T(8,128)(2,1)S(1)}, u32[]{:S(2)}, u32[]{:S(2)}) collective-permute-start(bf16[128,128]{1,0:T(8,128)(2,1)S(1)} %get-tuple-element.21), channel_id=1, source_target_pairs={{0,64},{64,128},{128,192},{192,256},{256,320},{320,384},{384,448},... | collective-permute-start | bytes 98312 | tf_op jit(solution)/shard_map/ppermute | solution.py:292
  72.2 5.8 %collective-permute-start.8 = (bf16[128,128]{1,0:T(8,128)(2,1)S(1)}, bf16[128,128]{1,0:T(8,128)(2,1)S(1)}, u32[]{:S(2)}, u32[]{:S(2)}) collective-permute-start(bf16[128,128]{1,0:T(8,128)(2,1)S(1)} %get-tuple-element.23), channel_id=1, source_target_pairs={{64,0},{128,64},{192,128},{256,192},{320,256},{384,320},{448,384},... | collective-permute-start | bytes 98312 | tf_op jit(solution)/shard_map/ppermute | solution.py:292
  86.4 17.5 %collective-permute-start.11 = (bf16[40,3072]{1,0:T(8,128)(2,1)S(1)}, bf16[40,3072]{1,0:T(8,128)(2,1)S(1)}, u32[]{:S(2)}, u32[]{:S(2)}) collective-permute-start(bf16[40,3072]{1,0:T(8,128)(2,1)S(1)} %get-tuple-element.28), channel_id=1, source_target_pairs={{0,56},{1,9},{2,58},{3,11},{4,60},{5,13},{6,62},{7,15},{8,0},{9,17... | collective-permute-start | bytes 737288 | tf_op jit(solution)/shard_map/ppermute | solution.py:309
  89.0 14.9 %collective-permute-start.12 = (bf16[40,3072]{1,0:T(8,128)(2,1)S(1)}, bf16[40,3072]{1,0:T(8,128)(2,1)S(1)}, u32[]{:S(2)}, u32[]{:S(2)}) collective-permute-start(bf16[40,3072]{1,0:T(8,128)(2,1)S(1)} %get-tuple-element.27), channel_id=1, source_target_pairs={{0,8},{1,57},{2,10},{3,59},{4,12},{5,61},{6,14},{7,63},{8,16},{9,1... | collective-permute-start | bytes 737288 | tf_op jit(solution)/shard_map/ppermute | solution.py:309
  92.2 12.1 %collective-permute-start.13 = (bf16[40,3072]{1,0:T(8,128)(2,1)S(1)}, bf16[40,3072]{1,0:T(8,128)(2,1)S(1)}, u32[]{:S(2)}, u32[]{:S(2)}) collective-permute-start(bf16[40,3072]{1,0:T(8,128)(2,1)S(1)} %get-tuple-element.26), channel_id=1, source_target_pairs={{0,16},{1,49},{2,18},{3,51},{4,20},{5,53},{6,22},{7,55},{8,24},{9,... | collective-permute-start | bytes 737288 | tf_op jit(solution)/shard_map/ppermute | solution.py:309
  98.0 15.0 %collective-permute-start.10 = (bf16[40,3072]{1,0:T(8,128)(2,1)S(1)}, bf16[40,3072]{1,0:T(8,128)(2,1)S(1)}, u32[]{:S(2)}, u32[]{:S(2)}) collective-permute-start(bf16[40,3072]{1,0:T(8,128)(2,1)S(1)} %get-tuple-element.30), channel_id=1, source_target_pairs={{0,56},{1,9},{2,58},{3,11},{4,60},{5,13},{6,62},{7,15},{8,0},{9,17... | collective-permute-start | bytes 737288 | tf_op jit(solution)/shard_map/ppermute | solution.py:309
  99.9 13.0 %collective-permute-start.9 = (bf16[40,3072]{1,0:T(8,128)(2,1)S(1)}, bf16[40,3072]{1,0:T(8,128)(2,1)S(1)}, u32[]{:S(2)}, u32[]{:S(2)}) collective-permute-start(bf16[40,3072]{1,0:T(8,128)(2,1)S(1)} %get-tuple-element.25), channel_id=1, source_target_pairs={{0,8},{1,57},{2,10},{3,59},{4,12},{5,61},{6,14},{7,63},{8,16},{9,1... | collective-permute-start | bytes 737288 | tf_op jit(solution)/shard_map/ppermute | solution.py:309
  104.4 14.0 %collective-permute-start.14 = (bf16[40,3072]{1,0:T(8,128)(2,1)S(1)}, bf16[40,3072]{1,0:T(8,128)(2,1)S(1)}, u32[]{:S(2)}, u32[]{:S(2)}) collective-permute-start(bf16[40,3072]{1,0:T(8,128)(2,1)S(1)} %add_convert_fusion.1), channel_id=1, source_target_pairs={{0,16},{1,49},{2,18},{3,51},{4,20},{5,53},{6,22},{7,55},{8,24},{9,... | collective-permute-start | bytes 737288 | tf_op jit(solution)/shard_map/ppermute | solution.py:309
  111.0 12.8 %collective-permute-start.15 = (bf16[40,3072]{1,0:T(8,128)(2,1)S(1)}, bf16[40,3072]{1,0:T(8,128)(2,1)S(1)}, u32[]{:S(2)}, u32[]{:S(2)}) collective-permute-start(bf16[40,3072]{1,0:T(8,128)(2,1)S(1)} %add_convert_fusion.2), channel_id=1, source_target_pairs={{0,48},{1,17},{2,50},{3,19},{4,52},{5,21},{6,54},{7,23},{8,56},{9,... | collective-permute-start | bytes 737288 | tf_op jit(solution)/shard_map/ppermute | solution.py:309
  (3 other events, 22.6 us)
where the time goes:
time: 126 us; the launch traced here: 125 us
  starting transfers between devices  80 us (63%)
  Pallas kernels  15.5 us (12%)
  blocking collectives  14.4 us (11%)
  waiting for transfers between devices  13.2 us (10%)
    ppermute x14, starting transfers between devices, toward(): return lax.ppermute(block, ('tp', 'dp'), pairs)  49.9 us
    all_to_all x2, starting transfers between devices, copy_for_each(): return lax.all_to_all(copies, axis, split_axis=0, concat_axis=0, tiled=True)  24.9 us
    pallas_call x6, Pallas kernels, call(): pl.pallas_call(kernel, out_shape=out_shape, in_specs=specs or [VMEM] * le...  15.5 us
    all_to_all x1, blocking collectives, copy_for_each(): return lax.all_to_all(copies, axis, split_axis=0, concat_axis=0, tiled=True)  14.4 us
    ppermute x14, waiting for transfers between devices, toward(): return lax.ppermute(block, ('tp', 'dp'), pairs)  11.3 us
    ppermute x2, starting transfers between devices, shift(): return lax.ppermute(block, axis, pairs)  5.17 us
  transfers between devices with their start and end apart: 18, of which 5 were waited for; matrix products, arithmetic and copies ran while one was open for 0% of the time, Pallas kernels for 4%

commit v1 on v0

--- a/solution.py
+++ b/solution.py
@@ -237,35 +237,28 @@
     sinks = jnp.concatenate([jnp.full((own, 1), sink[h], jnp.float32) for h in range(heads)], axis=0)
     begin = lax.axis_index("sp") * rows
     total = lax.axis_size("sp") * rows
-    for block, offset in enumerate(row_offsets(own, rows // own)):
-        offset = pl.multiple_of(offset, 8)
-        near = rounded(padded[pl.ds(offset, span), :])
+    offsets = row_offsets(own, rows // own)
+
+    def scored(block):
+        offset = pl.multiple_of(offsets[block], 8)
+        keys = jnp.concatenate([rounded(padded[pl.ds(offset, span), :]), ctx[...]], axis=0)
         query = rounded(queries[block * heads * own : (block + 1) * heads * own, :])
-        near_scores = contract(query, near, 1)
-        ctx_scores = contract(query, ctx[...], 1)
+        scores = contract(query, keys, 1)
         token = begin - WINDOW + offset + column
         seen = in_reach & (token >= 0) & (token < total)
-        near_scores = jnp.where(
-            seen[None], near_scores.reshape(heads, own, span), MASK_VALUE
-        ).reshape(heads * own, span)
-        peak = jnp.maximum(
-            jnp.maximum(
-                jnp.max(near_scores, axis=1, keepdims=True),
-                jnp.max(ctx_scores, axis=1, keepdims=True),
-            ),
-            sinks,
-        )
-        near_exp = jnp.exp(near_scores - peak)
-        ctx_exp = jnp.exp(ctx_scores - peak)
-        denominator = (
-            jnp.sum(near_exp, axis=1, keepdims=True)
-            + jnp.sum(ctx_exp, axis=1, keepdims=True)
-            + jnp.exp(sinks - peak)
-        )
-        inverse = 1.0 / denominator
-        result = contract(rounded(near_exp * inverse), near) + contract(
-            rounded(ctx_exp * inverse), ctx[...]
-        )
+        near = jnp.where(seen[None], scores[:, :span].reshape(heads, own, span), MASK_VALUE)
+        scores = jnp.concatenate([near.reshape(heads * own, span), scores[:, span:]], axis=1)
+        return scores, keys
+
+    following = scored(0)
+    for block in range(rows // own):
+        scores, keys = following
+        if block + 1 < rows // own:
+            following = scored(block + 1)
+        peak = jnp.maximum(jnp.max(scores, axis=1, keepdims=True), sinks)
+        weights = jnp.exp(scores - peak)
+        denominator = jnp.sum(weights, axis=1, keepdims=True) + jnp.exp(sinks - peak)
+        result = contract(rounded(weights), keys) * (1.0 / denominator)
         here = slice(block * own, (block + 1) * own)
         for pair in range(heads // 2):
             even = result[2 * pair * own : (2 * pair + 1) * own, :]
@@ -310,25 +303,26 @@
 
 
 def gather_rows(latent):
+    ahead2 = toward(latent, -2)
+    ahead1 = toward(latent, -1)
     back2 = toward(latent, 2)
-    ahead2 = toward(latent, -2)
     back1 = toward(latent, 1)
-    ahead1 = toward(latent, -1)
     far = toward(back2, 2)
-    back3, ahead3 = toward(back2, 1), toward(ahead2, -1)
+    back3 = toward(back2, 1)
+    ahead3 = toward(ahead2, -1)
     return [(back3,), (back2,), (back1,), (latent,), (ahead1,), (ahead2,), (ahead3,), (far,)]
 
 
 def reduce_rows(block):
     far = toward(block(4), 2)
+    up3 = toward(block(3), 1)
     down3 = toward(block(-3), -1)
-    up3 = toward(block(3), 1)
-    minus_two = added(block(-2), down3)
-    down2 = toward(minus_two, -2)
-    ahead, _ = lax.optimization_barrier((block(2), minus_two))
-    up2 = toward(added(ahead, up3, far), 2)
+    down1 = toward(block(-1), -1)
+    two = added(block(2), up3, far)
+    up2 = toward(two, 2)
     up1 = toward(block(1), 1)
-    down1 = toward(block(-1), -1)
+    behind, _ = lax.optimization_barrier((block(-2), two))
+    down2 = toward(added(behind, down3), -2)
     total = block(0).astype(jnp.float32)
     for part in (up1, down1, up2, down2):
         total = total + part.astype(jnp.float32)

time: 126 us -> 124 us (0.984)
  the two profiles are of different devices: /device:TPU:52 before, /device:TPU:14 now
where the time goes in v1:
time: 124 us; the launch traced here: 123 us
  starting transfers between devices  77.4 us (62%)
  waiting for transfers between devices  18.3 us (15%)
  Pallas kernels  13.5 us (11%)
  blocking collectives  12.5 us (10%)
    ppermute x14, starting transfers between devices, toward(): return lax.ppermute(block, ('tp', 'dp'), pairs)  47.2 us
    all_to_all x2, starting transfers between devices, copy_for_each(): return lax.all_to_all(copies, axis, split_axis=0, concat_axis=0, tiled=True)  25 us
    ppermute x14, waiting for transfers between devices, toward(): return lax.ppermute(block, ('tp', 'dp'), pairs)  16.3 us
    pallas_call x6, Pallas kernels, call(): pl.pallas_call(kernel, out_shape=out_shape, in_specs=specs or [VMEM] * le...  13.5 us
    all_to_all x1, blocking collectives, copy_for_each(): return lax.all_to_all(copies, axis, split_axis=0, concat_axis=0, tiled=True)  12.5 us
    ppermute x2, starting transfers between devices, shift(): return lax.ppermute(block, axis, pairs)  5.17 us
  transfers between devices with their start and end apart: 18, of which 6 were waited for; matrix products, arithmetic and copies ran while one was open for 0% of the time, Pallas kernels for 4%

profile of v1, /device:TPU:14, one launch (start us, length us, event | category | flops | bytes accessed | tf_op | source)
XLA Modules:
  0.0 123.4 jit_solution(16610661401480119080)
XLA Ops:
  0.0 2.2 %shard_map.136 = (f32[12,5,384]{2,1,0:T(8,128)}, f32[320,128]{1,0:T(8,128)}, f32[320,128]{1,0:T(8,128)}) custom-call(f32[3072]{0:T(1024)} %refs_0_.1, f32[3072]{0:T(1024)} %refs_1_.1, bf16[256,384]{1,0:T(8,128)(2,1)} %refs_2_.1, bf16[256,384]{1,0:T(8,128)(2,1)} %refs_3_.2, bf16[256,384]{1,0:T(8,128)(2,1)} %refs_4_.1), custom_call_target="tpu_custom_call" | custom-call | flops 1000000000 | bytes 1000000 | tf_op jit(solution)/shard_map/pallas_call | solution.py:33
  2.2 15.2 %all-to-all-start = ((f32[12,5,384]{2,1,0:T(8,128)}), f32[12,5,384]{2,1,0:T(8,128)S(1)}, u32[]{:S(2)}, u32[]{:S(2)}) async-start(f32[12,5,384]{2,1,0:T(8,128)} %get-tuple-element.15), calls=%async_computation | async-start | bytes 294912 | tf_op jit(solution)/shard_map/all_to_all | solution.py:279
  17.4 4.6 %collective-permute-start = (bf16[40,3072]{1,0:T(8,128)(2,1)S(1)}, bf16[40,3072]{1,0:T(8,128)(2,1)S(1)}, u32[]{:S(2)}, u32[]{:S(2)}) collective-permute-start(bf16[40,3072]{1,0:T(8,128)(2,1)S(1)} %copy-done), channel_id=1, source_target_pairs={{0,16},{1,49},{2,18},{3,51},{4,20},{5,53},{6,22},{7,55},{8,24},{9,... | collective-permute-start | bytes 737288 | tf_op jit(solution)/shard_map/ppermute | solution.py:302
  22.0 3.5 %collective-permute-start.4 = (bf16[40,3072]{1,0:T(8,128)(2,1)S(1)}, bf16[40,3072]{1,0:T(8,128)(2,1)S(1)}, u32[]{:S(2)}, u32[]{:S(2)}) collective-permute-start(bf16[40,3072]{1,0:T(8,128)(2,1)S(1)} %copy-done), channel_id=1, source_target_pairs={{0,48},{1,17},{2,50},{3,19},{4,52},{5,21},{6,54},{7,23},{8,56},{9,... | collective-permute-start | bytes 737288 | tf_op jit(solution)/shard_map/ppermute | solution.py:302
  25.5 3.2 %collective-permute-start.2 = (bf16[40,3072]{1,0:T(8,128)(2,1)S(1)}, bf16[40,3072]{1,0:T(8,128)(2,1)S(1)}, u32[]{:S(2)}, u32[]{:S(2)}) collective-permute-start(bf16[40,3072]{1,0:T(8,128)(2,1)S(1)} %copy-done), channel_id=1, source_target_pairs={{0,8},{1,57},{2,10},{3,59},{4,12},{5,61},{6,14},{7,63},{8,16},{9,1... | collective-permute-start | bytes 737288 | tf_op jit(solution)/shard_map/ppermute | solution.py:302
  28.7 2.7 %collective-permute-start.3 = (bf16[40,3072]{1,0:T(8,128)(2,1)S(1)}, bf16[40,3072]{1,0:T(8,128)(2,1)S(1)}, u32[]{:S(2)}, u32[]{:S(2)}) collective-permute-start(bf16[40,3072]{1,0:T(8,128)(2,1)S(1)} %copy-done), channel_id=1, source_target_pairs={{0,56},{1,9},{2,58},{3,11},{4,60},{5,13},{6,62},{7,15},{8,0},{9,17... | collective-permute-start | bytes 737288 | tf_op jit(solution)/shard_map/ppermute | solution.py:302
  31.4 2.9 %collective-permute-done.refs_1_ = bf16[40,3072]{1,0:T(8,128)(2,1)S(1)} collective-permute-done((bf16[40,3072]{1,0:T(8,128)(2,1)S(1)}, bf16[40,3072]{1,0:T(8,128)(2,1)S(1)}, u32[]{:S(2)}, u32[]{:S(2)}) %collective-permute-start) | collective-permute-done | bytes 245792 | tf_op jit(solution)/shard_map/ppermute | solution.py:302
  34.2 3.3 %collective-permute-start.1 = (bf16[40,3072]{1,0:T(8,128)(2,1)S(1)}, bf16[40,3072]{1,0:T(8,128)(2,1)S(1)}, u32[]{:S(2)}, u32[]{:S(2)}) collective-permute-start(bf16[40,3072]{1,0:T(8,128)(2,1)S(1)} %collective-permute-done.refs_1_), channel_id=1, source_target_pairs={{0,8},{1,57},{2,10},{3,59},{4,12},{5,61},{6,14},{7,63},{8,16},{9,1... | collective-permute-start | bytes 737288 | tf_op jit(solution)/shard_map/ppermute | solution.py:302
  37.5 6.6 %collective-permute-start.6 = (bf16[40,3072]{1,0:T(8,128)(2,1)S(1)}, bf16[40,3072]{1,0:T(8,128)(2,1)S(1)}, u32[]{:S(2)}, u32[]{:S(2)}) collective-permute-start(bf16[40,3072]{1,0:T(8,128)(2,1)S(1)} %collective-permute-done.refs_1_), channel_id=1, source_target_pairs={{0,16},{1,49},{2,18},{3,51},{4,20},{5,53},{6,22},{7,55},{8,24},{9,... | collective-permute-start | bytes 737288 | tf_op jit(solution)/shard_map/ppermute | solution.py:302
  44.2 1.9 %collective-permute-start.5 = (bf16[40,3072]{1,0:T(8,128)(2,1)S(1)}, bf16[40,3072]{1,0:T(8,128)(2,1)S(1)}, u32[]{:S(2)}, u32[]{:S(2)}) collective-permute-start(bf16[40,3072]{1,0:T(8,128)(2,1)S(1)} %collective-permute-done.4.refs_5_), channel_id=1, source_target_pairs={{0,56},{1,9},{2,58},{3,11},{4,60},{5,13},{6,62},{7,15},{8,0},{9,17... | collective-permute-start | bytes 737288 | tf_op jit(solution)/shard_map/ppermute | solution.py:302
  46.2 12.5 %all_to_all.15.refs_8_.vectors = f32[8,5,384]{2,1,0:T(8,128)S(1)} all-to-all(f32[8,5,384]{2,1,0:T(8,128)S(1)} %shard_map.137), channel_id=1, replica_groups=mesh['sp'=12,'tp'=8,'dp'=8] {'tp'}, dimensions={0} | all-to-all | bytes 122880 | tf_op jit(solution)/shard_map/all_to_all | solution.py:279
  59.8 9.9 %all-to-all-start.2 = ((bf16[12,32,128]{2,1,0:T(8,128)(2,1)}), bf16[12,32,128]{2,1,0:T(8,128)(2,1)S(1)}, u32[]{:S(2)}, u32[]{:S(2)}) async-start(bf16[12,32,128]{2,1,0:T(8,128)(2,1)} %shard_map.140), calls=%async_computation.2 | async-start | bytes 196608 | tf_op jit(solution)/shard_map/all_to_all | solution.py:279
  71.2 3.9 %collective-permute-start.7 = (bf16[128,128]{1,0:T(8,128)(2,1)S(1)}, bf16[128,128]{1,0:T(8,128)(2,1)S(1)}, u32[]{:S(2)}, u32[]{:S(2)}) collective-permute-start(bf16[128,128]{1,0:T(8,128)(2,1)S(1)} %get-tuple-element.21), channel_id=1, source_target_pairs={{0,64},{64,128},{128,192},{192,256},{256,320},{320,384},{384,448},... | collective-permute-start | bytes 98312 | tf_op jit(solution)/shard_map/ppermute | solution.py:285
  76.4 2.9 %shard_map.139 = (f32[1920,128]{1,0:T(8,128)S(1)}, f32[320,384]{1,0:T(8,128)S(1)}) custom-call(bf16[320,3072]{1,0:T(8,128)(2,1)S(1)} %get-tuple-element.18.hidden, bf16[3072,384]{1,0:T(8,128)(2,1)S(1)} %copy-done.1, bf16[3072,384]{1,0:T(8,128)(2,1)} %w_gate.1, f32[320,128]{1,0:T(8,128)S(1)} %copy-done.7, f32[320,128]{1,0:T(8,128)S(1)} %copy-done.8), custom_call_target="tpu_custom_call" | custom-call | flops 2000000000 | bytes 1000000 | tf_op jit(solution)/shard_map/pallas_call | solution.py:33
  81.3 5.9 %shard_map.141 = bf16[320,3072]{1,0:T(8,128)(2,1)S(1)} custom-call(f32[6]{0:T(128)S(1)} %copy-done.6, f32[1920,128]{1,0:T(8,128)S(1)} %get-tuple-element.19.queries, f32[320,384]{1,0:T(8,128)S(1)} %get-tuple-element.20.gate, bf16[128,128]{1,0:T(8,128)(2,1)S(1)} %collective-permute-done.7.low, bf16[320,128]{1,0:T(8,128)(2,1)S(1)} %get-tuple-element.22.middle, ...), custom_call_target="tpu_custom_call" | custom-call | flops 3000000000 | bytes 1000000 | tf_op jit(solution)/shard_map/pallas_call | solution.py:33
  87.3 2.3 %collective-permute-start.11 = (bf16[40,3072]{1,0:T(8,128)(2,1)S(1)}, bf16[40,3072]{1,0:T(8,128)(2,1)S(1)}, u32[]{:S(2)}, u32[]{:S(2)}) collective-permute-start(bf16[40,3072]{1,0:T(8,128)(2,1)S(1)} %get-tuple-element.29), channel_id=1, source_target_pairs={{0,8},{1,57},{2,10},{3,59},{4,12},{5,61},{6,14},{7,63},{8,16},{9,1... | collective-permute-start | bytes 737288 | tf_op jit(solution)/shard_map/ppermute | solution.py:302
  89.7 2.2 %collective-permute-start.12 = (bf16[40,3072]{1,0:T(8,128)(2,1)S(1)}, bf16[40,3072]{1,0:T(8,128)(2,1)S(1)}, u32[]{:S(2)}, u32[]{:S(2)}) collective-permute-start(bf16[40,3072]{1,0:T(8,128)(2,1)S(1)} %get-tuple-element.28), channel_id=1, source_target_pairs={{0,16},{1,49},{2,18},{3,51},{4,20},{5,53},{6,22},{7,55},{8,24},{9,... | collective-permute-start | bytes 737288 | tf_op jit(solution)/shard_map/ppermute | solution.py:302
  91.8 3.6 %collective-permute-start.14 = (bf16[40,3072]{1,0:T(8,128)(2,1)S(1)}, bf16[40,3072]{1,0:T(8,128)(2,1)S(1)}, u32[]{:S(2)}, u32[]{:S(2)}) collective-permute-start(bf16[40,3072]{1,0:T(8,128)(2,1)S(1)} %get-tuple-element.26), channel_id=1, source_target_pairs={{0,56},{1,9},{2,58},{3,11},{4,60},{5,13},{6,62},{7,15},{8,0},{9,17... | collective-permute-start | bytes 737288 | tf_op jit(solution)/shard_map/ppermute | solution.py:302
  95.4 4.7 %collective-permute-start.10 = (bf16[40,3072]{1,0:T(8,128)(2,1)S(1)}, bf16[40,3072]{1,0:T(8,128)(2,1)S(1)}, u32[]{:S(2)}, u32[]{:S(2)}) collective-permute-start(bf16[40,3072]{1,0:T(8,128)(2,1)S(1)} %get-tuple-element.30), channel_id=1, source_target_pairs={{0,56},{1,9},{2,58},{3,11},{4,60},{5,13},{6,62},{7,15},{8,0},{9,17... | collective-permute-start | bytes 737288 | tf_op jit(solution)/shard_map/ppermute | solution.py:302
  102.1 8.1 %collective-permute-done.12 = bf16[40,3072]{1,0:T(8,128)(2,1)S(1)} collective-permute-done((bf16[40,3072]{1,0:T(8,128)(2,1)S(1)}, bf16[40,3072]{1,0:T(8,128)(2,1)S(1)}, u32[]{:S(2)}, u32[]{:S(2)}) %collective-permute-start.12) | collective-permute-done | bytes 245792 | tf_op jit(solution)/shard_map/ppermute | solution.py:302
  110.3 2.0 %collective-permute-start.15 = (bf16[40,3072]{1,0:T(8,128)(2,1)S(1)}, bf16[40,3072]{1,0:T(8,128)(2,1)S(1)}, u32[]{:S(2)}, u32[]{:S(2)}) collective-permute-start(bf16[40,3072]{1,0:T(8,128)(2,1)S(1)} %add_convert_fusion.1), channel_id=1, source_target_pairs={{0,48},{1,17},{2,50},{3,19},{4,52},{5,21},{6,54},{7,23},{8,56},{9,... | collective-permute-start | bytes 737288 | tf_op jit(solution)/shard_map/ppermute | solution.py:302
  112.3 4.8 %collective-permute-start.13 = (bf16[40,3072]{1,0:T(8,128)(2,1)S(1)}, bf16[40,3072]{1,0:T(8,128)(2,1)S(1)}, u32[]{:S(2)}, u32[]{:S(2)}) collective-permute-start(bf16[40,3072]{1,0:T(8,128)(2,1)S(1)} %add_convert_fusion.2), channel_id=1, source_target_pairs={{0,16},{1,49},{2,18},{3,51},{4,20},{5,53},{6,22},{7,55},{8,24},{9,... | collective-permute-start | bytes 737288 | tf_op jit(solution)/shard_map/ppermute | solution.py:302
  117.1 2.2 %collective-permute-done.15 = bf16[40,3072]{1,0:T(8,128)(2,1)S(1)} collective-permute-done((bf16[40,3072]{1,0:T(8,128)(2,1)S(1)}, bf16[40,3072]{1,0:T(8,128)(2,1)S(1)}, u32[]{:S(2)}, u32[]{:S(2)}) %collective-permute-start.15) | collective-permute-done | bytes 245792 | tf_op jit(solution)/shard_map/ppermute | solution.py:302
  119.3 3.2 %collective-permute-done.13 = bf16[40,3072]{1,0:T(8,128)(2,1)S(1)} collective-permute-done((bf16[40,3072]{1,0:T(8,128)(2,1)S(1)}, bf16[40,3072]{1,0:T(8,128)(2,1)S(1)}, u32[]{:S(2)}, u32[]{:S(2)}) %collective-permute-start.13) | collective-permute-done | bytes 245792 | tf_op jit(solution)/shard_map/ppermute | solution.py:302
  (42 shorter events, 9.0 us)
Async XLA Ops:
  0.0 17.3 %copy-start = (bf16[40,3072]{1,0:T(8,128)(2,1)S(1)}, bf16[40,3072]{1,0:T(8,128)(2,1)}, u32[]{:S(2)}) copy-start(bf16[40,3072]{1,0:T(8,128)(2,1)} %refs_3_.3) | copy-start | bytes 737284
  2.2 44.0 %all-to-all-start = ((f32[12,5,384]{2,1,0:T(8,128)}), f32[12,5,384]{2,1,0:T(8,128)S(1)}, u32[]{:S(2)}, u32[]{:S(2)}) async-start(f32[12,5,384]{2,1,0:T(8,128)} %get-tuple-element.15), calls=%async_computation | async-start | bytes 294912 | tf_op jit(solution)/shard_map/all_to_all | solution.py:279
  17.3 41.3 %copy-start.2 = (bf16[3072,64]{0,1:T(8,128)(2,1)S(1)}, bf16[3072,64]{0,1:T(8,128)(2,1)}, u32[]{:S(2)}) copy-start(bf16[3072,64]{0,1:T(8,128)(2,1)} %param.23) | copy-start | bytes 1179652
  17.4 41.3 %copy-start.3 = (bf16[3072,64]{0,1:T(8,128)(2,1)S(1)}, bf16[3072,64]{0,1:T(8,128)(2,1)}, u32[]{:S(2)}) copy-start(bf16[3072,64]{0,1:T(8,128)(2,1)} %param.24) | copy-start | bytes 1179652
  17.4 41.3 %copy-start.4 = (bf16[32,3072]{1,0:T(8,128)(2,1)S(1)}, bf16[32,3072]{1,0:T(8,128)(2,1)}, u32[]{:S(2)}) copy-start(bf16[32,3072]{1,0:T(8,128)(2,1)} %context.1) | copy-start | bytes 589828
  17.4 41.3 %copy-start.5 = (f32[3072]{0:T(1024)S(1)}, f32[3072]{0:T(1024)}, u32[]{:S(2)}) copy-start(f32[3072]{0:T(1024)} %param.21) | copy-start | bytes 36868
  17.4 16.8 %collective-permute-start = (bf16[40,3072]{1,0:T(8,128)(2,1)S(1)}, bf16[40,3072]{1,0:T(8,128)(2,1)S(1)}, u32[]{:S(2)}, u32[]{:S(2)}) collective-permute-start(bf16[40,3072]{1,0:T(8,128)(2,1)S(1)} %copy-done), channel_id=1, source_target_pairs={{0,16},{1,49},{2,18},{3,51},{4,20},{5,53},{6,22},{7,55},{8,24},{9,... | collective-permute-start | bytes 737288 | tf_op jit(solution)/shard_map/ppermute | solution.py:302
  22.0 22.2 %collective-permute-start.4 = (bf16[40,3072]{1,0:T(8,128)(2,1)S(1)}, bf16[40,3072]{1,0:T(8,128)(2,1)S(1)}, u32[]{:S(2)}, u32[]{:S(2)}) collective-permute-start(bf16[40,3072]{1,0:T(8,128)(2,1)S(1)} %copy-done), channel_id=1, source_target_pairs={{0,48},{1,17},{2,50},{3,19},{4,52},{5,21},{6,54},{7,23},{8,56},{9,... | collective-permute-start | bytes 737288 | tf_op jit(solution)/shard_map/ppermute | solution.py:302
  25.5 44.2 %collective-permute-start.2 = (bf16[40,3072]{1,0:T(8,128)(2,1)S(1)}, bf16[40,3072]{1,0:T(8,128)(2,1)S(1)}, u32[]{:S(2)}, u32[]{:S(2)}) collective-permute-start(bf16[40,3072]{1,0:T(8,128)(2,1)S(1)} %copy-done), channel_id=1, source_target_pairs={{0,8},{1,57},{2,10},{3,59},{4,12},{5,61},{6,14},{7,63},{8,16},{9,1... | collective-permute-start | bytes 737288 | tf_op jit(solution)/shard_map/ppermute | solution.py:302
  28.7 41.0 %collective-permute-start.3 = (bf16[40,3072]{1,0:T(8,128)(2,1)S(1)}, bf16[40,3072]{1,0:T(8,128)(2,1)S(1)}, u32[]{:S(2)}, u32[]{:S(2)}) collective-permute-start(bf16[40,3072]{1,0:T(8,128)(2,1)S(1)} %copy-done), channel_id=1, source_target_pairs={{0,56},{1,9},{2,58},{3,11},{4,60},{5,13},{6,62},{7,15},{8,0},{9,17... | collective-permute-start | bytes 737288 | tf_op jit(solution)/shard_map/ppermute | solution.py:302
  34.2 35.5 %collective-permute-start.1 = (bf16[40,3072]{1,0:T(8,128)(2,1)S(1)}, bf16[40,3072]{1,0:T(8,128)(2,1)S(1)}, u32[]{:S(2)}, u32[]{:S(2)}) collective-permute-start(bf16[40,3072]{1,0:T(8,128)(2,1)S(1)} %collective-permute-done.refs_1_), channel_id=1, source_target_pairs={{0,8},{1,57},{2,10},{3,59},{4,12},{5,61},{6,14},{7,63},{8,16},{9,1... | collective-permute-start | bytes 737288 | tf_op jit(solution)/shard_map/ppermute | solution.py:302
  37.5 32.2 %collective-permute-start.6 = (bf16[40,3072]{1,0:T(8,128)(2,1)S(1)}, bf16[40,3072]{1,0:T(8,128)(2,1)S(1)}, u32[]{:S(2)}, u32[]{:S(2)}) collective-permute-start(bf16[40,3072]{1,0:T(8,128)(2,1)S(1)} %collective-permute-done.refs_1_), channel_id=1, source_target_pairs={{0,16},{1,49},{2,18},{3,51},{4,20},{5,53},{6,22},{7,55},{8,24},{9,... | collective-permute-start | bytes 737288 | tf_op jit(solution)/shard_map/ppermute | solution.py:302
  44.2 25.5 %collective-permute-start.5 = (bf16[40,3072]{1,0:T(8,128)(2,1)S(1)}, bf16[40,3072]{1,0:T(8,128)(2,1)S(1)}, u32[]{:S(2)}, u32[]{:S(2)}) collective-permute-start(bf16[40,3072]{1,0:T(8,128)(2,1)S(1)} %collective-permute-done.4.refs_5_), channel_id=1, source_target_pairs={{0,56},{1,9},{2,58},{3,11},{4,60},{5,13},{6,62},{7,15},{8,0},{9,17... | collective-permute-start | bytes 737288 | tf_op jit(solution)/shard_map/ppermute | solution.py:302
  58.6 11.1 %copy-start.8 = (f32[320,128]{1,0:T(8,128)S(1)}, f32[320,128]{1,0:T(8,128)}, u32[]{:S(2)}) copy-start(f32[320,128]{1,0:T(8,128)} %get-tuple-element.17.refs_13_.sine) | copy-start | bytes 491524
  59.8 21.5 %all-to-all-start.2 = ((bf16[12,32,128]{2,1,0:T(8,128)(2,1)}), bf16[12,32,128]{2,1,0:T(8,128)(2,1)S(1)}, u32[]{:S(2)}, u32[]{:S(2)}) async-start(bf16[12,32,128]{2,1,0:T(8,128)(2,1)} %shard_map.140), calls=%async_computation.2 | async-start | bytes 196608 | tf_op jit(solution)/shard_map/all_to_all | solution.py:279
  71.2 8.1 %collective-permute-start.7 = (bf16[128,128]{1,0:T(8,128)(2,1)S(1)}, bf16[128,128]{1,0:T(8,128)(2,1)S(1)}, u32[]{:S(2)}, u32[]{:S(2)}) collective-permute-start(bf16[128,128]{1,0:T(8,128)(2,1)S(1)} %get-tuple-element.21), channel_id=1, source_target_pairs={{0,64},{64,128},{128,192},{192,256},{256,320},{320,384},{384,448},... | collective-permute-start | bytes 98312 | tf_op jit(solution)/shard_map/ppermute | solution.py:285
  75.1 5.8 %collective-permute-start.8 = (bf16[128,128]{1,0:T(8,128)(2,1)S(1)}, bf16[128,128]{1,0:T(8,128)(2,1)S(1)}, u32[]{:S(2)}, u32[]{:S(2)}) collective-permute-start(bf16[128,128]{1,0:T(8,128)(2,1)S(1)} %get-tuple-element.23), channel_id=1, source_target_pairs={{64,0},{128,64},{192,128},{256,192},{320,256},{384,320},{448,384},... | collective-permute-start | bytes 98312 | tf_op jit(solution)/shard_map/ppermute | solution.py:285
  87.3 14.7 %collective-permute-start.11 = (bf16[40,3072]{1,0:T(8,128)(2,1)S(1)}, bf16[40,3072]{1,0:T(8,128)(2,1)S(1)}, u32[]{:S(2)}, u32[]{:S(2)}) collective-permute-start(bf16[40,3072]{1,0:T(8,128)(2,1)S(1)} %get-tuple-element.29), channel_id=1, source_target_pairs={{0,8},{1,57},{2,10},{3,59},{4,12},{5,61},{6,14},{7,63},{8,16},{9,1... | collective-permute-start | bytes 737288 | tf_op jit(solution)/shard_map/ppermute | solution.py:302
  89.7 20.5 %collective-permute-start.12 = (bf16[40,3072]{1,0:T(8,128)(2,1)S(1)}, bf16[40,3072]{1,0:T(8,128)(2,1)S(1)}, u32[]{:S(2)}, u32[]{:S(2)}) collective-permute-start(bf16[40,3072]{1,0:T(8,128)(2,1)S(1)} %get-tuple-element.28), channel_id=1, source_target_pairs={{0,16},{1,49},{2,18},{3,51},{4,20},{5,53},{6,22},{7,55},{8,24},{9,... | collective-permute-start | bytes 737288 | tf_op jit(solution)/shard_map/ppermute | solution.py:302
  91.8 18.4 %collective-permute-start.14 = (bf16[40,3072]{1,0:T(8,128)(2,1)S(1)}, bf16[40,3072]{1,0:T(8,128)(2,1)S(1)}, u32[]{:S(2)}, u32[]{:S(2)}) collective-permute-start(bf16[40,3072]{1,0:T(8,128)(2,1)S(1)} %get-tuple-element.26), channel_id=1, source_target_pairs={{0,56},{1,9},{2,58},{3,11},{4,60},{5,13},{6,62},{7,15},{8,0},{9,17... | collective-permute-start | bytes 737288 | tf_op jit(solution)/shard_map/ppermute | solution.py:302
  95.4 21.7 %collective-permute-start.10 = (bf16[40,3072]{1,0:T(8,128)(2,1)S(1)}, bf16[40,3072]{1,0:T(8,128)(2,1)S(1)}, u32[]{:S(2)}, u32[]{:S(2)}) collective-permute-start(bf16[40,3072]{1,0:T(8,128)(2,1)S(1)} %get-tuple-element.30), channel_id=1, source_target_pairs={{0,56},{1,9},{2,58},{3,11},{4,60},{5,13},{6,62},{7,15},{8,0},{9,17... | collective-permute-start | bytes 737288 | tf_op jit(solution)/shard_map/ppermute | solution.py:302
  100.1 17.0 %collective-permute-start.9 = (bf16[40,3072]{1,0:T(8,128)(2,1)S(1)}, bf16[40,3072]{1,0:T(8,128)(2,1)S(1)}, u32[]{:S(2)}, u32[]{:S(2)}) collective-permute-start(bf16[40,3072]{1,0:T(8,128)(2,1)S(1)} %get-tuple-element.25), channel_id=1, source_target_pairs={{0,8},{1,57},{2,10},{3,59},{4,12},{5,61},{6,14},{7,63},{8,16},{9,1... | collective-permute-start | bytes 737288 | tf_op jit(solution)/shard_map/ppermute | solution.py:302
  110.3 9.0 %collective-permute-start.15 = (bf16[40,3072]{1,0:T(8,128)(2,1)S(1)}, bf16[40,3072]{1,0:T(8,128)(2,1)S(1)}, u32[]{:S(2)}, u32[]{:S(2)}) collective-permute-start(bf16[40,3072]{1,0:T(8,128)(2,1)S(1)} %add_convert_fusion.1), channel_id=1, source_target_pairs={{0,48},{1,17},{2,50},{3,19},{4,52},{5,21},{6,54},{7,23},{8,56},{9,... | collective-permute-start | bytes 737288 | tf_op jit(solution)/shard_map/ppermute | solution.py:302
  112.3 10.2 %collective-permute-start.13 = (bf16[40,3072]{1,0:T(8,128)(2,1)S(1)}, bf16[40,3072]{1,0:T(8,128)(2,1)S(1)}, u32[]{:S(2)}, u32[]{:S(2)}) collective-permute-start(bf16[40,3072]{1,0:T(8,128)(2,1)S(1)} %add_convert_fusion.2), channel_id=1, source_target_pairs={{0,16},{1,49},{2,18},{3,51},{4,20},{5,53},{6,22},{7,55},{8,24},{9,... | collective-permute-start | bytes 737288 | tf_op jit(solution)/shard_map/ppermute | solution.py:302
  (3 other events, 22.7 us)

commit v2 on v1

--- a/solution.py
+++ b/solution.py
@@ -303,26 +303,25 @@
 
 
 def gather_rows(latent):
+    back2 = toward(latent, 2)
     ahead2 = toward(latent, -2)
+    back1 = toward(latent, 1)
     ahead1 = toward(latent, -1)
-    back2 = toward(latent, 2)
-    back1 = toward(latent, 1)
     far = toward(back2, 2)
-    back3 = toward(back2, 1)
-    ahead3 = toward(ahead2, -1)
+    back3, ahead3 = toward(back2, 1), toward(ahead2, -1)
     return [(back3,), (back2,), (back1,), (latent,), (ahead1,), (ahead2,), (ahead3,), (far,)]
 
 
 def reduce_rows(block):
     far = toward(block(4), 2)
+    down3 = toward(block(-3), -1)
     up3 = toward(block(3), 1)
-    down3 = toward(block(-3), -1)
+    minus_two = added(block(-2), down3)
+    down2 = toward(minus_two, -2)
+    ahead, _ = lax.optimization_barrier((block(2), minus_two))
+    up2 = toward(added(ahead, up3, far), 2)
+    up1 = toward(block(1), 1)
     down1 = toward(block(-1), -1)
-    two = added(block(2), up3, far)
-    up2 = toward(two, 2)
-    up1 = toward(block(1), 1)
-    behind, _ = lax.optimization_barrier((block(-2), two))
-    down2 = toward(added(behind, down3), -2)
     total = block(0).astype(jnp.float32)
     for part in (up1, down1, up2, down2):
         total = total + part.astype(jnp.float32)

time: 124 us -> 124 us (level)
  the two profiles are of different devices: /device:TPU:14 before, /device:TPU:48 now
where the time goes in v2:
time: 124 us; the launch traced here: 123 us
  starting transfers between devices  80 us (65%)
  blocking collectives  14.4 us (12%)
  Pallas kernels  13.5 us (11%)
  waiting for transfers between devices  13.2 us (11%)
    ppermute x14, starting transfers between devices, toward(): return lax.ppermute(block, ('tp', 'dp'), pairs)  49.9 us
    all_to_all x2, starting transfers between devices, copy_for_each(): return lax.all_to_all(copies, axis, split_axis=0, concat_axis=0, tiled=True)  24.9 us
    all_to_all x1, blocking collectives, copy_for_each(): return lax.all_to_all(copies, axis, split_axis=0, concat_axis=0, tiled=True)  14.4 us
    pallas_call x6, Pallas kernels, call(): pl.pallas_call(kernel, out_shape=out_shape, in_specs=specs or [VMEM] * le...  13.5 us
    ppermute x14, waiting for transfers between devices, toward(): return lax.ppermute(block, ('tp', 'dp'), pairs)  11.3 us
    ppermute x2, starting transfers between devices, shift(): return lax.ppermute(block, axis, pairs)  5.17 us
  transfers between devices with their start and end apart: 18, of which 5 were waited for; matrix products, arithmetic and copies ran while one was open for 0% of the time, Pallas kernels for 4%

profile of v2, /device:TPU:48, one launch (start us, length us, event | category | flops | bytes accessed | tf_op | source)
XLA Modules:
  0.0 122.7 jit_solution(7526085968914846482)
XLA Ops:
  0.0 2.2 %shard_map.136 = (f32[12,5,384]{2,1,0:T(8,128)}, f32[320,128]{1,0:T(8,128)}, f32[320,128]{1,0:T(8,128)}) custom-call(f32[3072]{0:T(1024)} %refs_0_.1, f32[3072]{0:T(1024)} %refs_1_.1, bf16[256,384]{1,0:T(8,128)(2,1)} %refs_2_.1, bf16[256,384]{1,0:T(8,128)(2,1)} %refs_3_.2, bf16[256,384]{1,0:T(8,128)(2,1)} %refs_4_.1), custom_call_target="tpu_custom_call" | custom-call | flops 1000000000 | bytes 1000000 | tf_op jit(solution)/shard_map/pallas_call | solution.py:33
  2.2 15.2 %all-to-all-start = ((f32[12,5,384]{2,1,0:T(8,128)}), f32[12,5,384]{2,1,0:T(8,128)S(1)}, u32[]{:S(2)}, u32[]{:S(2)}) async-start(f32[12,5,384]{2,1,0:T(8,128)} %get-tuple-element.15), calls=%async_computation | async-start | bytes 294912 | tf_op jit(solution)/shard_map/all_to_all | solution.py:279
  17.4 2.1 %collective-permute-start = (bf16[40,3072]{1,0:T(8,128)(2,1)S(1)}, bf16[40,3072]{1,0:T(8,128)(2,1)S(1)}, u32[]{:S(2)}, u32[]{:S(2)}) collective-permute-start(bf16[40,3072]{1,0:T(8,128)(2,1)S(1)} %copy-done), channel_id=1, source_target_pairs={{0,16},{1,49},{2,18},{3,51},{4,20},{5,53},{6,22},{7,55},{8,24},{9,... | collective-permute-start | bytes 737288 | tf_op jit(solution)/shard_map/ppermute | solution.py:302
  19.5 4.8 %collective-permute-start.4 = (bf16[40,3072]{1,0:T(8,128)(2,1)S(1)}, bf16[40,3072]{1,0:T(8,128)(2,1)S(1)}, u32[]{:S(2)}, u32[]{:S(2)}) collective-permute-start(bf16[40,3072]{1,0:T(8,128)(2,1)S(1)} %copy-done), channel_id=1, source_target_pairs={{0,48},{1,17},{2,50},{3,19},{4,52},{5,21},{6,54},{7,23},{8,56},{9,... | collective-permute-start | bytes 737288 | tf_op jit(solution)/shard_map/ppermute | solution.py:302
  24.3 2.6 %collective-permute-start.2 = (bf16[40,3072]{1,0:T(8,128)(2,1)S(1)}, bf16[40,3072]{1,0:T(8,128)(2,1)S(1)}, u32[]{:S(2)}, u32[]{:S(2)}) collective-permute-start(bf16[40,3072]{1,0:T(8,128)(2,1)S(1)} %copy-done), channel_id=1, source_target_pairs={{0,8},{1,57},{2,10},{3,59},{4,12},{5,61},{6,14},{7,63},{8,16},{9,1... | collective-permute-start | bytes 737288 | tf_op jit(solution)/shard_map/ppermute | solution.py:302
  26.9 3.8 %collective-permute-start.3 = (bf16[40,3072]{1,0:T(8,128)(2,1)S(1)}, bf16[40,3072]{1,0:T(8,128)(2,1)S(1)}, u32[]{:S(2)}, u32[]{:S(2)}) collective-permute-start(bf16[40,3072]{1,0:T(8,128)(2,1)S(1)} %copy-done), channel_id=1, source_target_pairs={{0,56},{1,9},{2,58},{3,11},{4,60},{5,13},{6,62},{7,15},{8,0},{9,17... | collective-permute-start | bytes 737288 | tf_op jit(solution)/shard_map/ppermute | solution.py:302
  30.7 4.7 %collective-permute-start.1 = (bf16[40,3072]{1,0:T(8,128)(2,1)S(1)}, bf16[40,3072]{1,0:T(8,128)(2,1)S(1)}, u32[]{:S(2)}, u32[]{:S(2)}) collective-permute-start(bf16[40,3072]{1,0:T(8,128)(2,1)S(1)} %collective-permute-done.refs_1_), channel_id=1, source_target_pairs={{0,8},{1,57},{2,10},{3,59},{4,12},{5,61},{6,14},{7,63},{8,16},{9,1... | collective-permute-start | bytes 737288 | tf_op jit(solution)/shard_map/ppermute | solution.py:302
  35.4 4.1 %collective-permute-start.6 = (bf16[40,3072]{1,0:T(8,128)(2,1)S(1)}, bf16[40,3072]{1,0:T(8,128)(2,1)S(1)}, u32[]{:S(2)}, u32[]{:S(2)}) collective-permute-start(bf16[40,3072]{1,0:T(8,128)(2,1)S(1)} %collective-permute-done.refs_1_), channel_id=1, source_target_pairs={{0,16},{1,49},{2,18},{3,51},{4,20},{5,53},{6,22},{7,55},{8,24},{9,... | collective-permute-start | bytes 737288 | tf_op jit(solution)/shard_map/ppermute | solution.py:302
  39.5 1.9 %collective-permute-start.5 = (bf16[40,3072]{1,0:T(8,128)(2,1)S(1)}, bf16[40,3072]{1,0:T(8,128)(2,1)S(1)}, u32[]{:S(2)}, u32[]{:S(2)}) collective-permute-start(bf16[40,3072]{1,0:T(8,128)(2,1)S(1)} %collective-permute-done.4.refs_5_), channel_id=1, source_target_pairs={{0,56},{1,9},{2,58},{3,11},{4,60},{5,13},{6,62},{7,15},{8,0},{9,17... | collective-permute-start | bytes 737288 | tf_op jit(solution)/shard_map/ppermute | solution.py:302
  41.5 14.4 %all_to_all.15.refs_8_.vectors = f32[8,5,384]{2,1,0:T(8,128)S(1)} all-to-all(f32[8,5,384]{2,1,0:T(8,128)S(1)} %shard_map.137), channel_id=1, replica_groups=mesh['sp'=12,'tp'=8,'dp'=8] {'tp'}, dimensions={0} | all-to-all | bytes 122880 | tf_op jit(solution)/shard_map/all_to_all | solution.py:279
  57.0 9.7 %all-to-all-start.2 = ((bf16[12,32,128]{2,1,0:T(8,128)(2,1)}), bf16[12,32,128]{2,1,0:T(8,128)(2,1)S(1)}, u32[]{:S(2)}, u32[]{:S(2)}) async-start(bf16[12,32,128]{2,1,0:T(8,128)(2,1)} %shard_map.140), calls=%async_computation.2 | async-start | bytes 196608 | tf_op jit(solution)/shard_map/all_to_all | solution.py:279
  68.3 3.9 %collective-permute-start.7 = (bf16[128,128]{1,0:T(8,128)(2,1)S(1)}, bf16[128,128]{1,0:T(8,128)(2,1)S(1)}, u32[]{:S(2)}, u32[]{:S(2)}) collective-permute-start(bf16[128,128]{1,0:T(8,128)(2,1)S(1)} %get-tuple-element.21), channel_id=1, source_target_pairs={{0,64},{64,128},{128,192},{192,256},{256,320},{320,384},{384,448},... | collective-permute-start | bytes 98312 | tf_op jit(solution)/shard_map/ppermute | solution.py:285
  73.5 2.9 %shard_map.139 = (f32[1920,128]{1,0:T(8,128)S(1)}, f32[320,384]{1,0:T(8,128)S(1)}) custom-call(bf16[320,3072]{1,0:T(8,128)(2,1)S(1)} %get-tuple-element.18.hidden, bf16[3072,384]{1,0:T(8,128)(2,1)S(1)} %copy-done.1, bf16[3072,384]{1,0:T(8,128)(2,1)} %w_gate.1, f32[320,128]{1,0:T(8,128)S(1)} %copy-done.7, f32[320,128]{1,0:T(8,128)S(1)} %copy-done.8), custom_call_target="tpu_custom_call" | custom-call | flops 2000000000 | bytes 1000000 | tf_op jit(solution)/shard_map/pallas_call | solution.py:33
  76.4 1.6 %collective-permute-done.8.high = bf16[128,128]{1,0:T(8,128)(2,1)S(1)} collective-permute-done((bf16[128,128]{1,0:T(8,128)(2,1)S(1)}, bf16[128,128]{1,0:T(8,128)(2,1)S(1)}, u32[]{:S(2)}, u32[]{:S(2)}) %collective-permute-start.8) | collective-permute-done | bytes 32800 | tf_op jit(solution)/shard_map/ppermute | solution.py:285
  78.4 5.9 %shard_map.141 = bf16[320,3072]{1,0:T(8,128)(2,1)S(1)} custom-call(f32[6]{0:T(128)S(1)} %copy-done.6, f32[1920,128]{1,0:T(8,128)S(1)} %get-tuple-element.19.queries, f32[320,384]{1,0:T(8,128)S(1)} %get-tuple-element.20.gate, bf16[128,128]{1,0:T(8,128)(2,1)S(1)} %collective-permute-done.7.low, bf16[320,128]{1,0:T(8,128)(2,1)S(1)} %get-tuple-element.22.middle, ...), custom_call_target="tpu_custom_call" | custom-call | flops 3000000000 | bytes 1000000 | tf_op jit(solution)/shard_map/pallas_call | solution.py:33
  84.4 2.6 %collective-permute-start.11 = (bf16[40,3072]{1,0:T(8,128)(2,1)S(1)}, bf16[40,3072]{1,0:T(8,128)(2,1)S(1)}, u32[]{:S(2)}, u32[]{:S(2)}) collective-permute-start(bf16[40,3072]{1,0:T(8,128)(2,1)S(1)} %get-tuple-element.28), channel_id=1, source_target_pairs={{0,56},{1,9},{2,58},{3,11},{4,60},{5,13},{6,62},{7,15},{8,0},{9,17... | collective-permute-start | bytes 737288 | tf_op jit(solution)/shard_map/ppermute | solution.py:302
  87.0 3.2 %collective-permute-start.12 = (bf16[40,3072]{1,0:T(8,128)(2,1)S(1)}, bf16[40,3072]{1,0:T(8,128)(2,1)S(1)}, u32[]{:S(2)}, u32[]{:S(2)}) collective-permute-start(bf16[40,3072]{1,0:T(8,128)(2,1)S(1)} %get-tuple-element.27), channel_id=1, source_target_pairs={{0,8},{1,57},{2,10},{3,59},{4,12},{5,61},{6,14},{7,63},{8,16},{9,1... | collective-permute-start | bytes 737288 | tf_op jit(solution)/shard_map/ppermute | solution.py:302
  90.2 5.8 %collective-permute-start.13 = (bf16[40,3072]{1,0:T(8,128)(2,1)S(1)}, bf16[40,3072]{1,0:T(8,128)(2,1)S(1)}, u32[]{:S(2)}, u32[]{:S(2)}) collective-permute-start(bf16[40,3072]{1,0:T(8,128)(2,1)S(1)} %get-tuple-element.26), channel_id=1, source_target_pairs={{0,16},{1,49},{2,18},{3,51},{4,20},{5,53},{6,22},{7,55},{8,24},{9,... | collective-permute-start | bytes 737288 | tf_op jit(solution)/shard_map/ppermute | solution.py:302
  96.0 1.9 %collective-permute-start.10 = (bf16[40,3072]{1,0:T(8,128)(2,1)S(1)}, bf16[40,3072]{1,0:T(8,128)(2,1)S(1)}, u32[]{:S(2)}, u32[]{:S(2)}) collective-permute-start(bf16[40,3072]{1,0:T(8,128)(2,1)S(1)} %get-tuple-element.30), channel_id=1, source_target_pairs={{0,56},{1,9},{2,58},{3,11},{4,60},{5,13},{6,62},{7,15},{8,0},{9,17... | collective-permute-start | bytes 737288 | tf_op jit(solution)/shard_map/ppermute | solution.py:302
  98.0 3.9 %collective-permute-start.9 = (bf16[40,3072]{1,0:T(8,128)(2,1)S(1)}, bf16[40,3072]{1,0:T(8,128)(2,1)S(1)}, u32[]{:S(2)}, u32[]{:S(2)}) collective-permute-start(bf16[40,3072]{1,0:T(8,128)(2,1)S(1)} %get-tuple-element.25), channel_id=1, source_target_pairs={{0,8},{1,57},{2,10},{3,59},{4,12},{5,61},{6,14},{7,63},{8,16},{9,1... | collective-permute-start | bytes 737288 | tf_op jit(solution)/shard_map/ppermute | solution.py:302
  102.5 6.6 %collective-permute-start.14 = (bf16[40,3072]{1,0:T(8,128)(2,1)S(1)}, bf16[40,3072]{1,0:T(8,128)(2,1)S(1)}, u32[]{:S(2)}, u32[]{:S(2)}) collective-permute-start(bf16[40,3072]{1,0:T(8,128)(2,1)S(1)} %add_convert_fusion.1), channel_id=1, source_target_pairs={{0,16},{1,49},{2,18},{3,51},{4,20},{5,53},{6,22},{7,55},{8,24},{9,... | collective-permute-start | bytes 737288 | tf_op jit(solution)/shard_map/ppermute | solution.py:302
  109.1 1.9 %collective-permute-start.15 = (bf16[40,3072]{1,0:T(8,128)(2,1)S(1)}, bf16[40,3072]{1,0:T(8,128)(2,1)S(1)}, u32[]{:S(2)}, u32[]{:S(2)}) collective-permute-start(bf16[40,3072]{1,0:T(8,128)(2,1)S(1)} %add_convert_fusion.2), channel_id=1, source_target_pairs={{0,48},{1,17},{2,50},{3,19},{4,52},{5,21},{6,54},{7,23},{8,56},{9,... | collective-permute-start | bytes 737288 | tf_op jit(solution)/shard_map/ppermute | solution.py:302
  111.0 5.3 %collective-permute-done.14 = bf16[40,3072]{1,0:T(8,128)(2,1)S(1)} collective-permute-done((bf16[40,3072]{1,0:T(8,128)(2,1)S(1)}, bf16[40,3072]{1,0:T(8,128)(2,1)S(1)}, u32[]{:S(2)}, u32[]{:S(2)}) %collective-permute-start.14) | collective-permute-done | bytes 245792 | tf_op jit(solution)/shard_map/ppermute | solution.py:302
  116.3 5.5 %collective-permute-done.15 = bf16[40,3072]{1,0:T(8,128)(2,1)S(1)} collective-permute-done((bf16[40,3072]{1,0:T(8,128)(2,1)S(1)}, bf16[40,3072]{1,0:T(8,128)(2,1)S(1)}, u32[]{:S(2)}, u32[]{:S(2)}) %collective-permute-start.15) | collective-permute-done | bytes 245792 | tf_op jit(solution)/shard_map/ppermute | solution.py:302
  (42 shorter events, 5.9 us)
Async XLA Ops:
  0.0 17.3 %copy-start = (bf16[40,3072]{1,0:T(8,128)(2,1)S(1)}, bf16[40,3072]{1,0:T(8,128)(2,1)}, u32[]{:S(2)}) copy-start(bf16[40,3072]{1,0:T(8,128)(2,1)} %refs_3_.3) | copy-start | bytes 737284
  2.2 39.3 %all-to-all-start = ((f32[12,5,384]{2,1,0:T(8,128)}), f32[12,5,384]{2,1,0:T(8,128)S(1)}, u32[]{:S(2)}, u32[]{:S(2)}) async-start(f32[12,5,384]{2,1,0:T(8,128)} %get-tuple-element.15), calls=%async_computation | async-start | bytes 294912 | tf_op jit(solution)/shard_map/all_to_all | solution.py:279
  17.3 38.5 %copy-start.2 = (bf16[3072,64]{0,1:T(8,128)(2,1)S(1)}, bf16[3072,64]{0,1:T(8,128)(2,1)}, u32[]{:S(2)}) copy-start(bf16[3072,64]{0,1:T(8,128)(2,1)} %param.23) | copy-start | bytes 1179652
  17.4 38.5 %copy-start.3 = (bf16[3072,64]{0,1:T(8,128)(2,1)S(1)}, bf16[3072,64]{0,1:T(8,128)(2,1)}, u32[]{:S(2)}) copy-start(bf16[3072,64]{0,1:T(8,128)(2,1)} %param.24) | copy-start | bytes 1179652
  17.4 38.5 %copy-start.4 = (bf16[32,3072]{1,0:T(8,128)(2,1)S(1)}, bf16[32,3072]{1,0:T(8,128)(2,1)}, u32[]{:S(2)}) copy-start(bf16[32,3072]{1,0:T(8,128)(2,1)} %context.1) | copy-start | bytes 589828
  17.4 38.5 %copy-start.5 = (f32[3072]{0:T(1024)S(1)}, f32[3072]{0:T(1024)}, u32[]{:S(2)}) copy-start(f32[3072]{0:T(1024)} %param.21) | copy-start | bytes 36868
  17.4 13.3 %collective-permute-start = (bf16[40,3072]{1,0:T(8,128)(2,1)S(1)}, bf16[40,3072]{1,0:T(8,128)(2,1)S(1)}, u32[]{:S(2)}, u32[]{:S(2)}) collective-permute-start(bf16[40,3072]{1,0:T(8,128)(2,1)S(1)} %copy-done), channel_id=1, source_target_pairs={{0,16},{1,49},{2,18},{3,51},{4,20},{5,53},{6,22},{7,55},{8,24},{9,... | collective-permute-start | bytes 737288 | tf_op jit(solution)/shard_map/ppermute | solution.py:302
  19.5 20.0 %collective-permute-start.4 = (bf16[40,3072]{1,0:T(8,128)(2,1)S(1)}, bf16[40,3072]{1,0:T(8,128)(2,1)S(1)}, u32[]{:S(2)}, u32[]{:S(2)}) collective-permute-start(bf16[40,3072]{1,0:T(8,128)(2,1)S(1)} %copy-done), channel_id=1, source_target_pairs={{0,48},{1,17},{2,50},{3,19},{4,52},{5,21},{6,54},{7,23},{8,56},{9,... | collective-permute-start | bytes 737288 | tf_op jit(solution)/shard_map/ppermute | solution.py:302
  24.3 42.4 %collective-permute-start.2 = (bf16[40,3072]{1,0:T(8,128)(2,1)S(1)}, bf16[40,3072]{1,0:T(8,128)(2,1)S(1)}, u32[]{:S(2)}, u32[]{:S(2)}) collective-permute-start(bf16[40,3072]{1,0:T(8,128)(2,1)S(1)} %copy-done), channel_id=1, source_target_pairs={{0,8},{1,57},{2,10},{3,59},{4,12},{5,61},{6,14},{7,63},{8,16},{9,1... | collective-permute-start | bytes 737288 | tf_op jit(solution)/shard_map/ppermute | solution.py:302
  26.9 39.9 %collective-permute-start.3 = (bf16[40,3072]{1,0:T(8,128)(2,1)S(1)}, bf16[40,3072]{1,0:T(8,128)(2,1)S(1)}, u32[]{:S(2)}, u32[]{:S(2)}) collective-permute-start(bf16[40,3072]{1,0:T(8,128)(2,1)S(1)} %copy-done), channel_id=1, source_target_pairs={{0,56},{1,9},{2,58},{3,11},{4,60},{5,13},{6,62},{7,15},{8,0},{9,17... | collective-permute-start | bytes 737288 | tf_op jit(solution)/shard_map/ppermute | solution.py:302
  30.7 36.0 %collective-permute-start.1 = (bf16[40,3072]{1,0:T(8,128)(2,1)S(1)}, bf16[40,3072]{1,0:T(8,128)(2,1)S(1)}, u32[]{:S(2)}, u32[]{:S(2)}) collective-permute-start(bf16[40,3072]{1,0:T(8,128)(2,1)S(1)} %collective-permute-done.refs_1_), channel_id=1, source_target_pairs={{0,8},{1,57},{2,10},{3,59},{4,12},{5,61},{6,14},{7,63},{8,16},{9,1... | collective-permute-start | bytes 737288 | tf_op jit(solution)/shard_map/ppermute | solution.py:302
  35.4 31.3 %collective-permute-start.6 = (bf16[40,3072]{1,0:T(8,128)(2,1)S(1)}, bf16[40,3072]{1,0:T(8,128)(2,1)S(1)}, u32[]{:S(2)}, u32[]{:S(2)}) collective-permute-start(bf16[40,3072]{1,0:T(8,128)(2,1)S(1)} %collective-permute-done.refs_1_), channel_id=1, source_target_pairs={{0,16},{1,49},{2,18},{3,51},{4,20},{5,53},{6,22},{7,55},{8,24},{9,... | collective-permute-start | bytes 737288 | tf_op jit(solution)/shard_map/ppermute | solution.py:302
  39.5 27.3 %collective-permute-start.5 = (bf16[40,3072]{1,0:T(8,128)(2,1)S(1)}, bf16[40,3072]{1,0:T(8,128)(2,1)S(1)}, u32[]{:S(2)}, u32[]{:S(2)}) collective-permute-start(bf16[40,3072]{1,0:T(8,128)(2,1)S(1)} %collective-permute-done.4.refs_5_), channel_id=1, source_target_pairs={{0,56},{1,9},{2,58},{3,11},{4,60},{5,13},{6,62},{7,15},{8,0},{9,17... | collective-permute-start | bytes 737288 | tf_op jit(solution)/shard_map/ppermute | solution.py:302
  55.8 10.9 %copy-start.8 = (f32[320,128]{1,0:T(8,128)S(1)}, f32[320,128]{1,0:T(8,128)}, u32[]{:S(2)}) copy-start(f32[320,128]{1,0:T(8,128)} %get-tuple-element.17.refs_13_.sine) | copy-start | bytes 491524
  57.0 21.4 %all-to-all-start.2 = ((bf16[12,32,128]{2,1,0:T(8,128)(2,1)}), bf16[12,32,128]{2,1,0:T(8,128)(2,1)S(1)}, u32[]{:S(2)}, u32[]{:S(2)}) async-start(bf16[12,32,128]{2,1,0:T(8,128)(2,1)} %shard_map.140), calls=%async_computation.2 | async-start | bytes 196608 | tf_op jit(solution)/shard_map/all_to_all | solution.py:279
  68.3 8.1 %collective-permute-start.7 = (bf16[128,128]{1,0:T(8,128)(2,1)S(1)}, bf16[128,128]{1,0:T(8,128)(2,1)S(1)}, u32[]{:S(2)}, u32[]{:S(2)}) collective-permute-start(bf16[128,128]{1,0:T(8,128)(2,1)S(1)} %get-tuple-element.21), channel_id=1, source_target_pairs={{0,64},{64,128},{128,192},{192,256},{256,320},{320,384},{384,448},... | collective-permute-start | bytes 98312 | tf_op jit(solution)/shard_map/ppermute | solution.py:285
  72.2 5.8 %collective-permute-start.8 = (bf16[128,128]{1,0:T(8,128)(2,1)S(1)}, bf16[128,128]{1,0:T(8,128)(2,1)S(1)}, u32[]{:S(2)}, u32[]{:S(2)}) collective-permute-start(bf16[128,128]{1,0:T(8,128)(2,1)S(1)} %get-tuple-element.23), channel_id=1, source_target_pairs={{64,0},{128,64},{192,128},{256,192},{320,256},{384,320},{448,384},... | collective-permute-start | bytes 98312 | tf_op jit(solution)/shard_map/ppermute | solution.py:285
  84.4 17.5 %collective-permute-start.11 = (bf16[40,3072]{1,0:T(8,128)(2,1)S(1)}, bf16[40,3072]{1,0:T(8,128)(2,1)S(1)}, u32[]{:S(2)}, u32[]{:S(2)}) collective-permute-start(bf16[40,3072]{1,0:T(8,128)(2,1)S(1)} %get-tuple-element.28), channel_id=1, source_target_pairs={{0,56},{1,9},{2,58},{3,11},{4,60},{5,13},{6,62},{7,15},{8,0},{9,17... | collective-permute-start | bytes 737288 | tf_op jit(solution)/shard_map/ppermute | solution.py:302
  87.0 15.0 %collective-permute-start.12 = (bf16[40,3072]{1,0:T(8,128)(2,1)S(1)}, bf16[40,3072]{1,0:T(8,128)(2,1)S(1)}, u32[]{:S(2)}, u32[]{:S(2)}) collective-permute-start(bf16[40,3072]{1,0:T(8,128)(2,1)S(1)} %get-tuple-element.27), channel_id=1, source_target_pairs={{0,8},{1,57},{2,10},{3,59},{4,12},{5,61},{6,14},{7,63},{8,16},{9,1... | collective-permute-start | bytes 737288 | tf_op jit(solution)/shard_map/ppermute | solution.py:302
  90.2 12.1 %collective-permute-start.13 = (bf16[40,3072]{1,0:T(8,128)(2,1)S(1)}, bf16[40,3072]{1,0:T(8,128)(2,1)S(1)}, u32[]{:S(2)}, u32[]{:S(2)}) collective-permute-start(bf16[40,3072]{1,0:T(8,128)(2,1)S(1)} %get-tuple-element.26), channel_id=1, source_target_pairs={{0,16},{1,49},{2,18},{3,51},{4,20},{5,53},{6,22},{7,55},{8,24},{9,... | collective-permute-start | bytes 737288 | tf_op jit(solution)/shard_map/ppermute | solution.py:302
  96.0 15.0 %collective-permute-start.10 = (bf16[40,3072]{1,0:T(8,128)(2,1)S(1)}, bf16[40,3072]{1,0:T(8,128)(2,1)S(1)}, u32[]{:S(2)}, u32[]{:S(2)}) collective-permute-start(bf16[40,3072]{1,0:T(8,128)(2,1)S(1)} %get-tuple-element.30), channel_id=1, source_target_pairs={{0,56},{1,9},{2,58},{3,11},{4,60},{5,13},{6,62},{7,15},{8,0},{9,17... | collective-permute-start | bytes 737288 | tf_op jit(solution)/shard_map/ppermute | solution.py:302
  98.0 13.1 %collective-permute-start.9 = (bf16[40,3072]{1,0:T(8,128)(2,1)S(1)}, bf16[40,3072]{1,0:T(8,128)(2,1)S(1)}, u32[]{:S(2)}, u32[]{:S(2)}) collective-permute-start(bf16[40,3072]{1,0:T(8,128)(2,1)S(1)} %get-tuple-element.25), channel_id=1, source_target_pairs={{0,8},{1,57},{2,10},{3,59},{4,12},{5,61},{6,14},{7,63},{8,16},{9,1... | collective-permute-start | bytes 737288 | tf_op jit(solution)/shard_map/ppermute | solution.py:302
  102.5 13.9 %collective-permute-start.14 = (bf16[40,3072]{1,0:T(8,128)(2,1)S(1)}, bf16[40,3072]{1,0:T(8,128)(2,1)S(1)}, u32[]{:S(2)}, u32[]{:S(2)}) collective-permute-start(bf16[40,3072]{1,0:T(8,128)(2,1)S(1)} %add_convert_fusion.1), channel_id=1, source_target_pairs={{0,16},{1,49},{2,18},{3,51},{4,20},{5,53},{6,22},{7,55},{8,24},{9,... | collective-permute-start | bytes 737288 | tf_op jit(solution)/shard_map/ppermute | solution.py:302
  109.1 12.8 %collective-permute-start.15 = (bf16[40,3072]{1,0:T(8,128)(2,1)S(1)}, bf16[40,3072]{1,0:T(8,128)(2,1)S(1)}, u32[]{:S(2)}, u32[]{:S(2)}) collective-permute-start(bf16[40,3072]{1,0:T(8,128)(2,1)S(1)} %add_convert_fusion.2), channel_id=1, source_target_pairs={{0,48},{1,17},{2,50},{3,19},{4,52},{5,21},{6,54},{7,23},{8,56},{9,... | collective-permute-start | bytes 737288 | tf_op jit(solution)/shard_map/ppermute | solution.py:302
  (3 other events, 22.6 us)

commit v3 on v2

--- a/solution.py
+++ b/solution.py
@@ -220,6 +220,7 @@
     *,
     own,
     span,
+    served,
 ):
     fetch = pltpu.make_async_copy(w_out, held, ready)
     fetch.start()
@@ -250,11 +251,11 @@
         scores = jnp.concatenate([near.reshape(heads * own, span), scores[:, span:]], axis=1)
         return scores, keys
 
-    following = scored(0)
-    for block in range(rows // own):
+    following = scored(served[0])
+    for at, block in enumerate(served):
         scores, keys = following
-        if block + 1 < rows // own:
-            following = scored(block + 1)
+        if at + 1 < len(served):
+            following = scored(served[at + 1])
         peak = jnp.maximum(jnp.max(scores, axis=1, keepdims=True), sinks)
         weights = jnp.exp(scores - peak)
         denominator = jnp.sum(weights, axis=1, keepdims=True) + jnp.exp(sinks - peak)
@@ -265,7 +266,7 @@
             odd = result[(2 * pair + 1) * own : (2 * pair + 2) * own, :]
             attended = jnp.where(lane < HEAD_SIZE, pltpu.roll(even, HEAD_SIZE, 1), odd)
             tile = gate[here, pair * LANES : (pair + 1) * LANES]
-            mixed[here, pair * LANES : (pair + 1) * LANES] = attended * (
+            mixed[at * own : (at + 1) * own, pair * LANES : (pair + 1) * LANES] = attended * (
                 tile / (1.0 + jnp.exp(-tile))
             )
     fetch.wait()
@@ -427,28 +428,37 @@
         grant=46,
     )
     span = 3 * LANES
-    product = call(
-        functools.partial(attend_kernel, own=own, span=span),
-        shape((rows, width), bf16),
-        sink_logit,
-        queries,
-        gate,
-        low,
-        key_value,
-        high,
-        ctx_all,
-        w_out,
-        specs=[SMEM] + [VMEM] * 6 + [HBM],
-        scratch=[
-            pltpu.VMEM((rows - own + span, LANES), f32),
-            pltpu.VMEM((rows, w_out.shape[0]), f32),
-            pltpu.VMEM(w_out.shape, bf16),
-            pltpu.SemaphoreType.DMA,
-        ],
-        flops=3 * 10**9,
-        grant=50,
-    )
-    branch = reduce_rows(lambda d: product[(d + behind) * own : (d + behind + 1) * own])
+
+    def attend(distances):
+        served = tuple(distance + behind for distance in distances)
+        product = call(
+            functools.partial(attend_kernel, own=own, span=span, served=served),
+            shape((own * len(served), width), bf16),
+            sink_logit,
+            queries,
+            gate,
+            low,
+            key_value,
+            high,
+            ctx_all,
+            w_out,
+            specs=[SMEM] + [VMEM] * 6 + [HBM],
+            scratch=[
+                pltpu.VMEM((rows - own + span, LANES), f32),
+                pltpu.VMEM((own * len(served), w_out.shape[0]), f32),
+                pltpu.VMEM(w_out.shape, bf16),
+                pltpu.SemaphoreType.DMA,
+            ],
+            flops=10**9,
+            grant=50,
+        )
+        return {
+            distance: product[at * own : (at + 1) * own] for at, distance in enumerate(distances)
+        }
+
+    product = attend((4, -3, 3))
+    product.update(attend((-2, 2, 1, 0, -1)))
+    branch = reduce_rows(product.__getitem__)
     lat_gate = vectors[:, 4, :].reshape(width)
     return rounded(latent.astype(f32) + lat_gate * branch)
 

time: 124 us -> 125 us (level)
  the two profiles are of different devices: /device:TPU:48 before, /device:TPU:6 now
where the time goes in v3:
time: 125 us; the launch traced here: 124 us
  starting transfers between devices  79.9 us (64%)
  Pallas kernels  14.9 us (12%)
  blocking collectives  14 us (11%)
  waiting for transfers between devices  12.5 us (10%)
    ppermute x14, starting transfers between devices, toward(): return lax.ppermute(block, ('tp', 'dp'), pairs)  49.7 us
    all_to_all x2, starting transfers between devices, copy_for_each(): return lax.all_to_all(copies, axis, split_axis=0, concat_axis=0, tiled=True)  25 us
    pallas_call x7, Pallas kernels, call(): pl.pallas_call(kernel, out_shape=out_shape, in_specs=specs or [VMEM] * le...  14.9 us
    all_to_all x1, blocking collectives, copy_for_each(): return lax.all_to_all(copies, axis, split_axis=0, concat_axis=0, tiled=True)  14 us
    ppermute x14, waiting for transfers between devices, toward(): return lax.ppermute(block, ('tp', 'dp'), pairs)  10.9 us
    ppermute x2, starting transfers between devices, shift(): return lax.ppermute(block, axis, pairs)  5.17 us
  transfers between devices with their start and end apart: 18, of which 4 were waited for; matrix products, arithmetic and copies ran while one was open for 0% of the time, Pallas kernels for 8%

profile of v3, /device:TPU:6, one launch (start us, length us, event | category | flops | bytes accessed | tf_op | source)
XLA Modules:
  0.0 124.1 jit_solution(11321743880324502576)
XLA Ops:
  0.0 2.2 %shard_map.136 = (f32[12,5,384]{2,1,0:T(8,128)}, f32[320,128]{1,0:T(8,128)}, f32[320,128]{1,0:T(8,128)}) custom-call(f32[3072]{0:T(1024)} %refs_0_.1, f32[3072]{0:T(1024)} %refs_1_.1, bf16[256,384]{1,0:T(8,128)(2,1)} %refs_2_.1, bf16[256,384]{1,0:T(8,128)(2,1)} %refs_3_.2, bf16[256,384]{1,0:T(8,128)(2,1)} %refs_4_.1), custom_call_target="tpu_custom_call" | custom-call | flops 1000000000 | bytes 1000000 | tf_op jit(solution)/shard_map/pallas_call | solution.py:33
  2.2 15.2 %all-to-all-start = ((f32[12,5,384]{2,1,0:T(8,128)}), f32[12,5,384]{2,1,0:T(8,128)S(1)}, u32[]{:S(2)}, u32[]{:S(2)}) async-start(f32[12,5,384]{2,1,0:T(8,128)} %get-tuple-element.15), calls=%async_computation | async-start | bytes 294912 | tf_op jit(solution)/shard_map/all_to_all | solution.py:280
  17.4 4.6 %collective-permute-start = (bf16[40,3072]{1,0:T(8,128)(2,1)S(1)}, bf16[40,3072]{1,0:T(8,128)(2,1)S(1)}, u32[]{:S(2)}, u32[]{:S(2)}) collective-permute-start(bf16[40,3072]{1,0:T(8,128)(2,1)S(1)} %copy-done), channel_id=1, source_target_pairs={{0,16},{1,49},{2,18},{3,51},{4,20},{5,53},{6,22},{7,55},{8,24},{9,... | collective-permute-start | bytes 737288 | tf_op jit(solution)/shard_map/ppermute | solution.py:303
  22.0 3.6 %collective-permute-start.4 = (bf16[40,3072]{1,0:T(8,128)(2,1)S(1)}, bf16[40,3072]{1,0:T(8,128)(2,1)S(1)}, u32[]{:S(2)}, u32[]{:S(2)}) collective-permute-start(bf16[40,3072]{1,0:T(8,128)(2,1)S(1)} %copy-done), channel_id=1, source_target_pairs={{0,48},{1,17},{2,50},{3,19},{4,52},{5,21},{6,54},{7,23},{8,56},{9,... | collective-permute-start | bytes 737288 | tf_op jit(solution)/shard_map/ppermute | solution.py:303
  25.6 3.4 %collective-permute-start.2 = (bf16[40,3072]{1,0:T(8,128)(2,1)S(1)}, bf16[40,3072]{1,0:T(8,128)(2,1)S(1)}, u32[]{:S(2)}, u32[]{:S(2)}) collective-permute-start(bf16[40,3072]{1,0:T(8,128)(2,1)S(1)} %copy-done), channel_id=1, source_target_pairs={{0,8},{1,57},{2,10},{3,59},{4,12},{5,61},{6,14},{7,63},{8,16},{9,1... | collective-permute-start | bytes 737288 | tf_op jit(solution)/shard_map/ppermute | solution.py:303
  29.0 3.7 %collective-permute-start.3 = (bf16[40,3072]{1,0:T(8,128)(2,1)S(1)}, bf16[40,3072]{1,0:T(8,128)(2,1)S(1)}, u32[]{:S(2)}, u32[]{:S(2)}) collective-permute-start(bf16[40,3072]{1,0:T(8,128)(2,1)S(1)} %copy-done), channel_id=1, source_target_pairs={{0,56},{1,9},{2,58},{3,11},{4,60},{5,13},{6,62},{7,15},{8,0},{9,17... | collective-permute-start | bytes 737288 | tf_op jit(solution)/shard_map/ppermute | solution.py:303
  32.7 5.0 %collective-permute-start.1 = (bf16[40,3072]{1,0:T(8,128)(2,1)S(1)}, bf16[40,3072]{1,0:T(8,128)(2,1)S(1)}, u32[]{:S(2)}, u32[]{:S(2)}) collective-permute-start(bf16[40,3072]{1,0:T(8,128)(2,1)S(1)} %collective-permute-done.refs_1_), channel_id=1, source_target_pairs={{0,8},{1,57},{2,10},{3,59},{4,12},{5,61},{6,14},{7,63},{8,16},{9,1... | collective-permute-start | bytes 737288 | tf_op jit(solution)/shard_map/ppermute | solution.py:303
  37.7 4.3 %collective-permute-start.6 = (bf16[40,3072]{1,0:T(8,128)(2,1)S(1)}, bf16[40,3072]{1,0:T(8,128)(2,1)S(1)}, u32[]{:S(2)}, u32[]{:S(2)}) collective-permute-start(bf16[40,3072]{1,0:T(8,128)(2,1)S(1)} %collective-permute-done.refs_1_), channel_id=1, source_target_pairs={{0,16},{1,49},{2,18},{3,51},{4,20},{5,53},{6,22},{7,55},{8,24},{9,... | collective-permute-start | bytes 737288 | tf_op jit(solution)/shard_map/ppermute | solution.py:303
  42.0 3.6 %collective-permute-start.5 = (bf16[40,3072]{1,0:T(8,128)(2,1)S(1)}, bf16[40,3072]{1,0:T(8,128)(2,1)S(1)}, u32[]{:S(2)}, u32[]{:S(2)}) collective-permute-start(bf16[40,3072]{1,0:T(8,128)(2,1)S(1)} %collective-permute-done.4.refs_5_), channel_id=1, source_target_pairs={{0,56},{1,9},{2,58},{3,11},{4,60},{5,13},{6,62},{7,15},{8,0},{9,17... | collective-permute-start | bytes 737288 | tf_op jit(solution)/shard_map/ppermute | solution.py:303
  45.7 14.0 %all_to_all.15.refs_8_.vectors = f32[8,5,384]{2,1,0:T(8,128)S(1)} all-to-all(f32[8,5,384]{2,1,0:T(8,128)S(1)} %shard_map.137), channel_id=1, replica_groups=mesh['sp'=12,'tp'=8,'dp'=8] {'tp'}, dimensions={0} | all-to-all | bytes 122880 | tf_op jit(solution)/shard_map/all_to_all | solution.py:280
  60.8 9.9 %all-to-all-start.2 = ((bf16[12,32,128]{2,1,0:T(8,128)(2,1)}), bf16[12,32,128]{2,1,0:T(8,128)(2,1)S(1)}, u32[]{:S(2)}, u32[]{:S(2)}) async-start(bf16[12,32,128]{2,1,0:T(8,128)(2,1)} %shard_map.140), calls=%async_computation.2 | async-start | bytes 196608 | tf_op jit(solution)/shard_map/all_to_all | solution.py:280
  73.3 3.9 %collective-permute-start.7 = (bf16[128,128]{1,0:T(8,128)(2,1)S(1)}, bf16[128,128]{1,0:T(8,128)(2,1)S(1)}, u32[]{:S(2)}, u32[]{:S(2)}) collective-permute-start(bf16[128,128]{1,0:T(8,128)(2,1)S(1)} %get-tuple-element.21), channel_id=1, source_target_pairs={{0,64},{64,128},{128,192},{192,256},{256,320},{320,384},{384,448},... | collective-permute-start | bytes 98312 | tf_op jit(solution)/shard_map/ppermute | solution.py:286
  78.5 2.9 %shard_map.139 = (f32[1920,128]{1,0:T(8,128)S(1)}, f32[320,384]{1,0:T(8,128)S(1)}) custom-call(bf16[320,3072]{1,0:T(8,128)(2,1)S(1)} %get-tuple-element.18.hidden, bf16[3072,384]{1,0:T(8,128)(2,1)S(1)} %copy-done.2, bf16[3072,384]{1,0:T(8,128)(2,1)} %w_gate.1, f32[320,128]{1,0:T(8,128)S(1)} %copy-done.8, f32[320,128]{1,0:T(8,128)S(1)} %copy-done.9), custom_call_target="tpu_custom_call" | custom-call | flops 2000000000 | bytes 1000000 | tf_op jit(solution)/shard_map/pallas_call | solution.py:33
  83.0 3.2 %shard_map.142 = bf16[120,3072]{1,0:T(8,128)(2,1)S(1)} custom-call(f32[6]{0:T(128)S(1)} %copy-done.1, f32[1920,128]{1,0:T(8,128)S(1)} %get-tuple-element.19.queries, f32[320,384]{1,0:T(8,128)S(1)} %get-tuple-element.20.gate, bf16[128,128]{1,0:T(8,128)(2,1)S(1)} %collective-permute-done.7.low, bf16[320,128]{1,0:T(8,128)(2,1)S(1)} %get-tuple-element.22.middle, ...), custom_call_target="tpu_custom_call" | custom-call | flops 1000000000 | bytes 1000000 | tf_op jit(solution)/shard_map/pallas_call | solution.py:33
  86.2 1.9 %collective-permute-start.11 = (bf16[40,3072]{1,0:T(8,128)(2,1)S(1)}, bf16[40,3072]{1,0:T(8,128)(2,1)S(1)}, u32[]{:S(2)}, u32[]{:S(2)}) collective-permute-start(bf16[40,3072]{1,0:T(8,128)(2,1)S(1)} %get-tuple-element.30), channel_id=1, source_target_pairs={{0,56},{1,9},{2,58},{3,11},{4,60},{5,13},{6,62},{7,15},{8,0},{9,17... | collective-permute-start | bytes 737288 | tf_op jit(solution)/shard_map/ppermute | solution.py:303
  88.1 3.9 %collective-permute-start.13 = (bf16[40,3072]{1,0:T(8,128)(2,1)S(1)}, bf16[40,3072]{1,0:T(8,128)(2,1)S(1)}, u32[]{:S(2)}, u32[]{:S(2)}) collective-permute-start(bf16[40,3072]{1,0:T(8,128)(2,1)S(1)} %get-tuple-element.29), channel_id=1, source_target_pairs={{0,16},{1,49},{2,18},{3,51},{4,20},{5,53},{6,22},{7,55},{8,24},{9,... | collective-permute-start | bytes 737288 | tf_op jit(solution)/shard_map/ppermute | solution.py:303
  92.1 2.3 %collective-permute-start.12 = (bf16[40,3072]{1,0:T(8,128)(2,1)S(1)}, bf16[40,3072]{1,0:T(8,128)(2,1)S(1)}, u32[]{:S(2)}, u32[]{:S(2)}) collective-permute-start(bf16[40,3072]{1,0:T(8,128)(2,1)S(1)} %get-tuple-element.28), channel_id=1, source_target_pairs={{0,8},{1,57},{2,10},{3,59},{4,12},{5,61},{6,14},{7,63},{8,16},{9,1... | collective-permute-start | bytes 737288 | tf_op jit(solution)/shard_map/ppermute | solution.py:303
  94.4 4.2 %shard_map.141 = bf16[200,3072]{1,0:T(8,128)(2,1)S(1)} custom-call(f32[6]{0:T(128)S(1)} %copy-done.1, f32[1920,128]{1,0:T(8,128)S(1)} %get-tuple-element.19.queries, f32[320,384]{1,0:T(8,128)S(1)} %get-tuple-element.20.gate, bf16[128,128]{1,0:T(8,128)(2,1)S(1)} %collective-permute-done.7.low, bf16[320,128]{1,0:T(8,128)(2,1)S(1)} %get-tuple-element.22.middle, ...), custom_call_target="tpu_custom_call" | custom-call | flops 1000000000 | bytes 1000000 | tf_op jit(solution)/shard_map/pallas_call | solution.py:33
  98.6 4.7 %collective-permute-start.10 = (bf16[40,3072]{1,0:T(8,128)(2,1)S(1)}, bf16[40,3072]{1,0:T(8,128)(2,1)S(1)}, u32[]{:S(2)}, u32[]{:S(2)}) collective-permute-start(bf16[40,3072]{1,0:T(8,128)(2,1)S(1)} %get-tuple-element.27), channel_id=1, source_target_pairs={{0,56},{1,9},{2,58},{3,11},{4,60},{5,13},{6,62},{7,15},{8,0},{9,17... | collective-permute-start | bytes 737288 | tf_op jit(solution)/shard_map/ppermute | solution.py:303
  103.4 1.9 %collective-permute-start.9 = (bf16[40,3072]{1,0:T(8,128)(2,1)S(1)}, bf16[40,3072]{1,0:T(8,128)(2,1)S(1)}, u32[]{:S(2)}, u32[]{:S(2)}) collective-permute-start(bf16[40,3072]{1,0:T(8,128)(2,1)S(1)} %get-tuple-element.25), channel_id=1, source_target_pairs={{0,8},{1,57},{2,10},{3,59},{4,12},{5,61},{6,14},{7,63},{8,16},{9,1... | collective-permute-start | bytes 737288 | tf_op jit(solution)/shard_map/ppermute | solution.py:303
  105.4 4.8 %collective-permute-start.15 = (bf16[40,3072]{1,0:T(8,128)(2,1)S(1)}, bf16[40,3072]{1,0:T(8,128)(2,1)S(1)}, u32[]{:S(2)}, u32[]{:S(2)}) collective-permute-start(bf16[40,3072]{1,0:T(8,128)(2,1)S(1)} %add_convert_fusion.2), channel_id=1, source_target_pairs={{0,48},{1,17},{2,50},{3,19},{4,52},{5,21},{6,54},{7,23},{8,56},{9,... | collective-permute-start | bytes 737288 | tf_op jit(solution)/shard_map/ppermute | solution.py:303
  110.3 1.9 %collective-permute-start.14 = (bf16[40,3072]{1,0:T(8,128)(2,1)S(1)}, bf16[40,3072]{1,0:T(8,128)(2,1)S(1)}, u32[]{:S(2)}, u32[]{:S(2)}) collective-permute-start(bf16[40,3072]{1,0:T(8,128)(2,1)S(1)} %add_convert_fusion.1), channel_id=1, source_target_pairs={{0,16},{1,49},{2,18},{3,51},{4,20},{5,53},{6,22},{7,55},{8,24},{9,... | collective-permute-start | bytes 737288 | tf_op jit(solution)/shard_map/ppermute | solution.py:303
  114.1 3.2 %collective-permute-done.15 = bf16[40,3072]{1,0:T(8,128)(2,1)S(1)} collective-permute-done((bf16[40,3072]{1,0:T(8,128)(2,1)S(1)}, bf16[40,3072]{1,0:T(8,128)(2,1)S(1)}, u32[]{:S(2)}, u32[]{:S(2)}) %collective-permute-start.15) | collective-permute-done | bytes 245792 | tf_op jit(solution)/shard_map/ppermute | solution.py:303
  117.3 5.8 %collective-permute-done.14 = bf16[40,3072]{1,0:T(8,128)(2,1)S(1)} collective-permute-done((bf16[40,3072]{1,0:T(8,128)(2,1)S(1)}, bf16[40,3072]{1,0:T(8,128)(2,1)S(1)}, u32[]{:S(2)}, u32[]{:S(2)}) %collective-permute-start.14) | collective-permute-done | bytes 245792 | tf_op jit(solution)/shard_map/ppermute | solution.py:303
  (46 shorter events, 9.6 us)
Async XLA Ops:
  0.0 17.3 %copy-start = (bf16[40,3072]{1,0:T(8,128)(2,1)S(1)}, bf16[40,3072]{1,0:T(8,128)(2,1)}, u32[]{:S(2)}) copy-start(bf16[40,3072]{1,0:T(8,128)(2,1)} %refs_3_.3) | copy-start | bytes 737284
  2.2 43.5 %all-to-all-start = ((f32[12,5,384]{2,1,0:T(8,128)}), f32[12,5,384]{2,1,0:T(8,128)S(1)}, u32[]{:S(2)}, u32[]{:S(2)}) async-start(f32[12,5,384]{2,1,0:T(8,128)} %get-tuple-element.15), calls=%async_computation | async-start | bytes 294912 | tf_op jit(solution)/shard_map/all_to_all | solution.py:280
  17.4 42.3 %copy-start.3 = (bf16[3072,64]{0,1:T(8,128)(2,1)S(1)}, bf16[3072,64]{0,1:T(8,128)(2,1)}, u32[]{:S(2)}) copy-start(bf16[3072,64]{0,1:T(8,128)(2,1)} %param.23) | copy-start | bytes 1179652
  17.4 42.3 %copy-start.4 = (bf16[3072,64]{0,1:T(8,128)(2,1)S(1)}, bf16[3072,64]{0,1:T(8,128)(2,1)}, u32[]{:S(2)}) copy-start(bf16[3072,64]{0,1:T(8,128)(2,1)} %param.24) | copy-start | bytes 1179652
  17.4 42.3 %copy-start.5 = (bf16[32,3072]{1,0:T(8,128)(2,1)S(1)}, bf16[32,3072]{1,0:T(8,128)(2,1)}, u32[]{:S(2)}) copy-start(bf16[32,3072]{1,0:T(8,128)(2,1)} %context.1) | copy-start | bytes 589828
  17.4 42.3 %copy-start.6 = (f32[3072]{0:T(1024)S(1)}, f32[3072]{0:T(1024)}, u32[]{:S(2)}) copy-start(f32[3072]{0:T(1024)} %param.21) | copy-start | bytes 36868
  17.4 15.3 %collective-permute-start = (bf16[40,3072]{1,0:T(8,128)(2,1)S(1)}, bf16[40,3072]{1,0:T(8,128)(2,1)S(1)}, u32[]{:S(2)}, u32[]{:S(2)}) collective-permute-start(bf16[40,3072]{1,0:T(8,128)(2,1)S(1)} %copy-done), channel_id=1, source_target_pairs={{0,16},{1,49},{2,18},{3,51},{4,20},{5,53},{6,22},{7,55},{8,24},{9,... | collective-permute-start | bytes 737288 | tf_op jit(solution)/shard_map/ppermute | solution.py:303
  22.0 20.0 %collective-permute-start.4 = (bf16[40,3072]{1,0:T(8,128)(2,1)S(1)}, bf16[40,3072]{1,0:T(8,128)(2,1)S(1)}, u32[]{:S(2)}, u32[]{:S(2)}) collective-permute-start(bf16[40,3072]{1,0:T(8,128)(2,1)S(1)} %copy-done), channel_id=1, source_target_pairs={{0,48},{1,17},{2,50},{3,19},{4,52},{5,21},{6,54},{7,23},{8,56},{9,... | collective-permute-start | bytes 737288 | tf_op jit(solution)/shard_map/ppermute | solution.py:303
  25.6 45.0 %collective-permute-start.2 = (bf16[40,3072]{1,0:T(8,128)(2,1)S(1)}, bf16[40,3072]{1,0:T(8,128)(2,1)S(1)}, u32[]{:S(2)}, u32[]{:S(2)}) collective-permute-start(bf16[40,3072]{1,0:T(8,128)(2,1)S(1)} %copy-done), channel_id=1, source_target_pairs={{0,8},{1,57},{2,10},{3,59},{4,12},{5,61},{6,14},{7,63},{8,16},{9,1... | collective-permute-start | bytes 737288 | tf_op jit(solution)/shard_map/ppermute | solution.py:303
  29.0 41.7 %collective-permute-start.3 = (bf16[40,3072]{1,0:T(8,128)(2,1)S(1)}, bf16[40,3072]{1,0:T(8,128)(2,1)S(1)}, u32[]{:S(2)}, u32[]{:S(2)}) collective-permute-start(bf16[40,3072]{1,0:T(8,128)(2,1)S(1)} %copy-done), channel_id=1, source_target_pairs={{0,56},{1,9},{2,58},{3,11},{4,60},{5,13},{6,62},{7,15},{8,0},{9,17... | collective-permute-start | bytes 737288 | tf_op jit(solution)/shard_map/ppermute | solution.py:303
  32.7 38.0 %collective-permute-start.1 = (bf16[40,3072]{1,0:T(8,128)(2,1)S(1)}, bf16[40,3072]{1,0:T(8,128)(2,1)S(1)}, u32[]{:S(2)}, u32[]{:S(2)}) collective-permute-start(bf16[40,3072]{1,0:T(8,128)(2,1)S(1)} %collective-permute-done.refs_1_), channel_id=1, source_target_pairs={{0,8},{1,57},{2,10},{3,59},{4,12},{5,61},{6,14},{7,63},{8,16},{9,1... | collective-permute-start | bytes 737288 | tf_op jit(solution)/shard_map/ppermute | solution.py:303
  37.7 33.0 %collective-permute-start.6 = (bf16[40,3072]{1,0:T(8,128)(2,1)S(1)}, bf16[40,3072]{1,0:T(8,128)(2,1)S(1)}, u32[]{:S(2)}, u32[]{:S(2)}) collective-permute-start(bf16[40,3072]{1,0:T(8,128)(2,1)S(1)} %collective-permute-done.refs_1_), channel_id=1, source_target_pairs={{0,16},{1,49},{2,18},{3,51},{4,20},{5,53},{6,22},{7,55},{8,24},{9,... | collective-permute-start | bytes 737288 | tf_op jit(solution)/shard_map/ppermute | solution.py:303
  42.0 28.7 %collective-permute-start.5 = (bf16[40,3072]{1,0:T(8,128)(2,1)S(1)}, bf16[40,3072]{1,0:T(8,128)(2,1)S(1)}, u32[]{:S(2)}, u32[]{:S(2)}) collective-permute-start(bf16[40,3072]{1,0:T(8,128)(2,1)S(1)} %collective-permute-done.4.refs_5_), channel_id=1, source_target_pairs={{0,56},{1,9},{2,58},{3,11},{4,60},{5,13},{6,62},{7,15},{8,0},{9,17... | collective-permute-start | bytes 737288 | tf_op jit(solution)/shard_map/ppermute | solution.py:303
  59.7 11.1 %copy-start.7 = (f32[320,128]{1,0:T(8,128)S(1)}, f32[320,128]{1,0:T(8,128)}, u32[]{:S(2)}) copy-start(f32[320,128]{1,0:T(8,128)} %get-tuple-element.16.refs_12_.cosine) | copy-start | bytes 491524
  60.8 22.2 %all-to-all-start.2 = ((bf16[12,32,128]{2,1,0:T(8,128)(2,1)}), bf16[12,32,128]{2,1,0:T(8,128)(2,1)S(1)}, u32[]{:S(2)}, u32[]{:S(2)}) async-start(bf16[12,32,128]{2,1,0:T(8,128)(2,1)} %shard_map.140), calls=%async_computation.2 | async-start | bytes 196608 | tf_op jit(solution)/shard_map/all_to_all | solution.py:280
  73.3 8.1 %collective-permute-start.7 = (bf16[128,128]{1,0:T(8,128)(2,1)S(1)}, bf16[128,128]{1,0:T(8,128)(2,1)S(1)}, u32[]{:S(2)}, u32[]{:S(2)}) collective-permute-start(bf16[128,128]{1,0:T(8,128)(2,1)S(1)} %get-tuple-element.21), channel_id=1, source_target_pairs={{0,64},{64,128},{128,192},{192,256},{256,320},{320,384},{384,448},... | collective-permute-start | bytes 98312 | tf_op jit(solution)/shard_map/ppermute | solution.py:286
  77.2 5.8 %collective-permute-start.8 = (bf16[128,128]{1,0:T(8,128)(2,1)S(1)}, bf16[128,128]{1,0:T(8,128)(2,1)S(1)}, u32[]{:S(2)}, u32[]{:S(2)}) collective-permute-start(bf16[128,128]{1,0:T(8,128)(2,1)S(1)} %get-tuple-element.23), channel_id=1, source_target_pairs={{64,0},{128,64},{192,128},{256,192},{320,256},{384,320},{448,384},... | collective-permute-start | bytes 98312 | tf_op jit(solution)/shard_map/ppermute | solution.py:286
  86.2 19.1 %collective-permute-start.11 = (bf16[40,3072]{1,0:T(8,128)(2,1)S(1)}, bf16[40,3072]{1,0:T(8,128)(2,1)S(1)}, u32[]{:S(2)}, u32[]{:S(2)}) collective-permute-start(bf16[40,3072]{1,0:T(8,128)(2,1)S(1)} %get-tuple-element.30), channel_id=1, source_target_pairs={{0,56},{1,9},{2,58},{3,11},{4,60},{5,13},{6,62},{7,15},{8,0},{9,17... | collective-permute-start | bytes 737288 | tf_op jit(solution)/shard_map/ppermute | solution.py:303
  88.1 22.1 %collective-permute-start.13 = (bf16[40,3072]{1,0:T(8,128)(2,1)S(1)}, bf16[40,3072]{1,0:T(8,128)(2,1)S(1)}, u32[]{:S(2)}, u32[]{:S(2)}) collective-permute-start(bf16[40,3072]{1,0:T(8,128)(2,1)S(1)} %get-tuple-element.29), channel_id=1, source_target_pairs={{0,16},{1,49},{2,18},{3,51},{4,20},{5,53},{6,22},{7,55},{8,24},{9,... | collective-permute-start | bytes 737288 | tf_op jit(solution)/shard_map/ppermute | solution.py:303
  92.1 18.2 %collective-permute-start.12 = (bf16[40,3072]{1,0:T(8,128)(2,1)S(1)}, bf16[40,3072]{1,0:T(8,128)(2,1)S(1)}, u32[]{:S(2)}, u32[]{:S(2)}) collective-permute-start(bf16[40,3072]{1,0:T(8,128)(2,1)S(1)} %get-tuple-element.28), channel_id=1, source_target_pairs={{0,8},{1,57},{2,10},{3,59},{4,12},{5,61},{6,14},{7,63},{8,16},{9,1... | collective-permute-start | bytes 737288 | tf_op jit(solution)/shard_map/ppermute | solution.py:303
  98.6 13.6 %collective-permute-start.10 = (bf16[40,3072]{1,0:T(8,128)(2,1)S(1)}, bf16[40,3072]{1,0:T(8,128)(2,1)S(1)}, u32[]{:S(2)}, u32[]{:S(2)}) collective-permute-start(bf16[40,3072]{1,0:T(8,128)(2,1)S(1)} %get-tuple-element.27), channel_id=1, source_target_pairs={{0,56},{1,9},{2,58},{3,11},{4,60},{5,13},{6,62},{7,15},{8,0},{9,17... | collective-permute-start | bytes 737288 | tf_op jit(solution)/shard_map/ppermute | solution.py:303
  103.4 10.8 %collective-permute-start.9 = (bf16[40,3072]{1,0:T(8,128)(2,1)S(1)}, bf16[40,3072]{1,0:T(8,128)(2,1)S(1)}, u32[]{:S(2)}, u32[]{:S(2)}) collective-permute-start(bf16[40,3072]{1,0:T(8,128)(2,1)S(1)} %get-tuple-element.25), channel_id=1, source_target_pairs={{0,8},{1,57},{2,10},{3,59},{4,12},{5,61},{6,14},{7,63},{8,16},{9,1... | collective-permute-start | bytes 737288 | tf_op jit(solution)/shard_map/ppermute | solution.py:303
  105.4 12.0 %collective-permute-start.15 = (bf16[40,3072]{1,0:T(8,128)(2,1)S(1)}, bf16[40,3072]{1,0:T(8,128)(2,1)S(1)}, u32[]{:S(2)}, u32[]{:S(2)}) collective-permute-start(bf16[40,3072]{1,0:T(8,128)(2,1)S(1)} %add_convert_fusion.2), channel_id=1, source_target_pairs={{0,48},{1,17},{2,50},{3,19},{4,52},{5,21},{6,54},{7,23},{8,56},{9,... | collective-permute-start | bytes 737288 | tf_op jit(solution)/shard_map/ppermute | solution.py:303
  110.3 12.8 %collective-permute-start.14 = (bf16[40,3072]{1,0:T(8,128)(2,1)S(1)}, bf16[40,3072]{1,0:T(8,128)(2,1)S(1)}, u32[]{:S(2)}, u32[]{:S(2)}) collective-permute-start(bf16[40,3072]{1,0:T(8,128)(2,1)S(1)} %add_convert_fusion.1), channel_id=1, source_target_pairs={{0,16},{1,49},{2,18},{3,51},{4,20},{5,53},{6,22},{7,55},{8,24},{9,... | collective-permute-start | bytes 737288 | tf_op jit(solution)/shard_map/ppermute | solution.py:303
  (4 other events, 21.2 us)
